TPU v7x, 256 devices: a whole 4x4x8 slice. The times are simulated.
256 devices in a mesh: sp: 64 (over z, y, core), tp: 4 (over x).
Axes of the slice: x: 4, y: 4, z: 8, core: 2. Of those that a mesh axis runs over, the one named last changes fastest.
Arguments:
- stream: bfloat16 [8192, 2048], P('sp'), may hold values from -12 to 12
- out_grad: bfloat16 [8192, 2048], P('sp'), may hold values from -16 to 16
- routes: int32 [8192, 2], P('sp'), may hold values from 0 to 63, all different within a row; in each aligned block of 128 rows (0 to 127, 128 to 255, ...) at most 8 rows name the same one
- route_weight: float32 [8192, 2], P('sp'), may hold values from 0.2 to 1
- queries: bfloat16 [8192, 8, 128], P('sp', 'tp'), may hold values from -6 to 6
- key_vectors: bfloat16 [8192, 8, 128], P('sp', 'tp'), may hold values from -6 to 6
- value_vectors: bfloat16 [8192, 8, 256], P('sp', 'tp'), may hold values from -6 to 6
- log_decay: float32 [8192, 8], P('sp', 'tp'), may hold values from -1 to 0
- out_proj: bfloat16 [2048, 2048], P(None, 'tp'), may hold values from -0.125 to 0.125
- gate_weight: bfloat16 [64, 2048, 1024], P('sp', None, 'tp'), may hold values from -0.125 to 0.125
- up_weight: bfloat16 [64, 2048, 1024], P('sp', None, 'tp'), may hold values from -0.125 to 0.125
- down_weight: bfloat16 [64, 1024, 2048], P('sp', 'tp'), may hold values from -0.1875 to 0.1875
Outputs:
- gate_grad: bfloat16 [64, 2048, 1024], P('sp', None, 'tp')
- up_grad: bfloat16 [64, 2048, 1024], P('sp', None, 'tp')
- down_grad: bfloat16 [64, 1024, 2048], P('sp', 'tp')
- proj_grad: float32 [2048, 2048], P('sp', 'tp')
- query_grad: bfloat16 [8192, 8, 128], P('sp', 'tp')
- key_grad: bfloat16 [8192, 8, 128], P('sp', 'tp')
- value_grad: bfloat16 [8192, 8, 256], P('sp', 'tp')
Inputs may be any that keep to these rules, and one draw needn't show every extreme that they name: `routes`: each row names two different experts. In each aligned block of 128 rows no expert is named by more than 8 rows, and in some block an expert is named by exactly 8.
All inputs are finite; a program needn't handle non-finite values.
Results may differ from a plain program's by a relative error of at most 0.025.
Values may be sent and summed in bfloat16 or wider, within the bound.
A program may use at most 128 MiB of HBM per device.

v0:
```python
import jax
import jax.numpy as jnp
from jax import lax
from jax.sharding import Mesh
from jax.sharding import PartitionSpec as P

SP = ("sp_0", "sp_1", "sp_2")


CLAMP_LIMIT = 7.0
GATE_SLOPE = 1.702
EPSILON = 1e-06
TOP_PRECISION = lax.Precision.HIGHEST


def in_one_piece(arrays, axis, split_dim, concat_dim, along):
    both = jnp.concatenate(arrays, axis=along)
    result, at, finished = (
        lax.all_to_all(both, axis, split_axis=split_dim, concat_axis=concat_dim, tiled=True),
        0,
        [],
    )
    for a in arrays:
        finished.append(lax.slice_in_dim(result, at, at + a.shape[along], axis=along))
        at += a.shape[along]
    return tuple(finished)


def split_up(x, dim, length):
    before, after = (x.shape[:dim], x.shape[dim + 1 :])
    return jnp.moveaxis(x.reshape(*before, length, -1, *after), dim, 0)


def sent_and_summed(x, axis, dim):
    pieces = split_up(x, dim, lax.axis_size(axis))
    arrived = lax.all_to_all(pieces, axis, split_axis=0, concat_axis=0, tiled=True)
    return arrived.astype(jnp.float32).sum(axis=0)


def copy_for_each(x, axis):
    copies = jnp.broadcast_to(x, (lax.axis_size(axis), *x.shape))
    return lax.all_to_all(copies, axis, split_axis=0, concat_axis=0, tiled=True)


def joined_along(pieces, dim):
    lengths = list(pieces.shape[1:])
    lengths[dim] *= pieces.shape[0]
    return jnp.moveaxis(pieces, 0, dim).reshape(lengths)


def collect(x, axis, dim):
    pieces = copy_for_each(x, axis)
    return joined_along(pieces, dim)


def filled_with(x, identity):
    return jax.tree.map(
        lambda a, e: jnp.broadcast_to(jnp.asarray(e, a.dtype), a.shape), x, identity
    )


def prefix_by_axis(x, axes, combine, identity):
    before = start = filled_with(x, identity)
    total = x
    for axis in reversed(axes):
        length, position = (lax.axis_size(axis), lax.axis_index(axis))
        pieces = jax.tree.map(
            lambda part, kind: lax.all_gather(part.astype(kind), axis),
            total,
            (jnp.bfloat16, jnp.bfloat16),
        )
        inside, total = (start, start)
        for k in range(length):
            passed = k < position
            total = combine(
                total, jax.tree.map(lambda part, own: part[k].astype(own.dtype), pieces, x)
            )
            inside = jax.tree.map(lambda new, old: jnp.where(passed, new, old), total, inside)
        before = combine(inside, before)
    return before


def summed_rows(total, axes):
    for axis in axes:
        total = lax.psum_scatter(total, axis, scatter_dimension=0, tiled=True)
    return total


def prefix_by_axis_2(x, axes, combine, identity):
    before = start = filled_with(x, identity)
    total = x
    for axis in reversed(axes):
        length, position = (lax.axis_size(axis), lax.axis_index(axis))
        pieces = jax.tree.map(
            lambda part, kind: lax.all_gather(part.astype(kind), axis),
            total,
            jax.tree.map(lambda a: jnp.bfloat16 if a.dtype == jnp.float32 else a.dtype, x),
        )
        inside, total = (start, start)
        for k in reversed(range(length)):
            passed = k > position
            total = combine(
                total, jax.tree.map(lambda part, own: part[k].astype(own.dtype), pieces, x)
            )
            inside = jax.tree.map(lambda new, old: jnp.where(passed, new, old), total, inside)
        before = combine(inside, before)
    return before


def slot_numbers(route_block, expert_count):
    flat_ids = route_block.reshape(-1)
    onehot = (flat_ids[:, None] == jnp.arange(expert_count, dtype=jnp.int32)[None, :]).astype(
        jnp.int32
    )
    before = jnp.cumsum(onehot, axis=0) - onehot
    return (flat_ids, jnp.sum(before * onehot, axis=1))


def rotation_tables(start, count, key_width):
    frequency = 1.0 / 10000.0 ** jnp.linspace(0.0, 1.0, key_width // 2, dtype=jnp.float32)
    token_position = (start + jnp.arange(count, dtype=jnp.int32)).astype(jnp.float32)
    angles = token_position[:, None] * frequency[None, :]
    return (jnp.cos(angles), jnp.sin(angles))


def turn(field, cosines, sines):
    paired = field.reshape(field.shape[:-1] + (field.shape[-1] // 2, 2))
    even_part = paired[..., 0]
    odd_part = paired[..., 1]
    cos_rows = cosines[:, None, :]
    sin_rows = sines[:, None, :]
    turned = jnp.stack(
        [even_part * cos_rows - odd_part * sin_rows, odd_part * cos_rows + even_part * sin_rows],
        axis=-1,
    )
    return turned.reshape(field.shape)


def decay_combine(earlier, next_rows):
    return (earlier[0] * next_rows[0], next_rows[1] + next_rows[0][:, None, None] * earlier[1])


def expert_local(routed_rows, routed_grads, gate_w, up_w, down_w):
    gate_pre = jnp.dot(routed_rows, gate_w, preferred_element_type=jnp.float32)
    up_pre = jnp.dot(routed_rows, up_w, preferred_element_type=jnp.float32)
    gate_clip = jnp.minimum(gate_pre, CLAMP_LIMIT)
    up_clip = jnp.clip(up_pre, -CLAMP_LIMIT, CLAMP_LIMIT)
    sigmoid_gate = jax.nn.sigmoid(GATE_SLOPE * gate_clip)
    activated = (gate_clip * sigmoid_gate * (up_clip + 1.0)).astype(jnp.bfloat16)
    down_part = lax.dot_general(
        activated, routed_grads, (((0,), (0,)), ((), ())), preferred_element_type=jnp.float32
    )
    act_grad = lax.dot_general(
        routed_grads, down_w, (((1,), (1,)), ((), ())), preferred_element_type=jnp.float32
    )
    slope = sigmoid_gate + GATE_SLOPE * gate_clip * sigmoid_gate * (1.0 - sigmoid_gate)
    gate_pre_grad = jnp.where(
        gate_pre < CLAMP_LIMIT, act_grad * (up_clip + 1.0) * slope, 0.0
    ).astype(jnp.bfloat16)
    up_pre_grad = jnp.where(
        jnp.abs(up_pre) < CLAMP_LIMIT, act_grad * gate_clip * sigmoid_gate, 0.0
    ).astype(jnp.bfloat16)
    gate_part = lax.dot_general(
        routed_rows, gate_pre_grad, (((0,), (0,)), ((), ())), preferred_element_type=jnp.float32
    )
    up_part = lax.dot_general(
        routed_rows, up_pre_grad, (((0,), (0,)), ((), ())), preferred_element_type=jnp.float32
    )
    back_rows = lax.dot_general(
        gate_pre_grad, gate_w, (((1,), (1,)), ((), ())), preferred_element_type=jnp.float32
    )
    back_rows = back_rows + lax.dot_general(
        up_pre_grad, up_w, (((1,), (1,)), ((), ())), preferred_element_type=jnp.float32
    )
    return (
        gate_part.astype(jnp.bfloat16),
        up_part.astype(jnp.bfloat16),
        down_part.astype(jnp.bfloat16),
        back_rows.astype(jnp.bfloat16),
    )


def per_device(
    stream,
    out_grad,
    routes,
    route_weight,
    queries,
    key_vectors,
    value_vectors,
    log_decay,
    out_proj,
    gate_weight,
    up_weight,
    down_weight,
):
    experts = lax.axis_size(SP)
    tokens_here = stream.shape[0]
    model_width = stream.shape[1]
    capacity = 4 * tokens_here // experts
    pair_count = 2 * tokens_here
    flat_ids, slot_ids = slot_numbers(routes, experts)
    destination = flat_ids * capacity + slot_ids
    source = (
        jnp.full((experts * capacity,), -1, jnp.int32)
        .at[destination]
        .set(jnp.arange(pair_count, dtype=jnp.int32))
    )
    present = (source >= 0)[:, None]
    picked = jnp.maximum(source, 0)
    zero_value = jnp.zeros((), jnp.bfloat16)
    pair_grad = (route_weight[:, :, None] * out_grad[:, None, :].astype(jnp.float32)).astype(
        jnp.bfloat16
    )
    pair_grad = pair_grad.reshape(pair_count, model_width)
    send_rows = jnp.where(present, jnp.take(stream, picked // 2, axis=0), zero_value)
    send_rows = send_rows.reshape(experts, capacity, model_width)
    send_grads = jnp.where(present, jnp.take(pair_grad, picked, axis=0), zero_value)
    send_grads = send_grads.reshape(experts, capacity, model_width)
    routed_rows, routed_grads = in_one_piece((send_rows, send_grads), SP, 0, 0, 1)
    routed_rows = routed_rows.reshape(experts * capacity, model_width)
    routed_grads = routed_grads.reshape(experts * capacity, model_width)
    gate_part, up_part, down_part, back_rows = expert_local(
        routed_rows, routed_grads, gate_weight[0], up_weight[0], down_weight[0]
    )
    shares = sent_and_summed(back_rows.reshape(experts, capacity, model_width), "tp", 2)
    shares = lax.all_to_all(
        shares.astype(jnp.bfloat16), SP, split_axis=0, concat_axis=0, tiled=True
    )
    returned = collect(shares, "tp", 2)
    returned = returned.reshape(experts * capacity, model_width)
    per_pair = (
        jnp.take(returned, destination, axis=0)
        .reshape(tokens_here, 2, model_width)
        .astype(jnp.float32)
    )
    resid_grad = (out_grad.astype(jnp.float32) + per_pair[:, 0] + per_pair[:, 1]).astype(
        jnp.bfloat16
    )
    heads_local = queries.shape[1]
    key_width = queries.shape[2]
    value_width = value_vectors.shape[2]
    key_scale = key_width ** (-0.5)
    cosines, sines = rotation_tables(lax.axis_index(SP) * tokens_here, tokens_here, key_width)
    query_rotated = turn(queries.astype(jnp.float32), cosines, sines).transpose(1, 0, 2)
    key_rotated = (turn(key_vectors.astype(jnp.float32), cosines, sines) * key_scale).transpose(
        1, 0, 2
    )
    value_per_head = value_vectors.astype(jnp.float32).transpose(1, 0, 2)
    running_total = jnp.cumsum(log_decay, axis=0).T
    block_total = running_total[:, -1]
    causal = (jnp.arange(tokens_here)[:, None] >= jnp.arange(tokens_here)[None, :])[None]
    difference = running_total[:, :, None] - running_total[:, None, :]
    decay_mask = jnp.where(causal, jnp.exp(jnp.where(causal, difference, 0.0)), 0.0)
    per_head_decay = jnp.exp(running_total)
    remaining_decay = jnp.exp(block_total[:, None] - running_total)
    carried = jnp.exp(block_total)
    inner_state = jnp.einsum(
        "wfs,wfi->wsi",
        key_rotated * remaining_decay[..., None],
        value_per_head,
        precision=TOP_PRECISION,
    )
    identity = (jnp.ones_like(carried), jnp.zeros_like(inner_state))
    incoming_state = prefix_by_axis((carried, inner_state), SP, decay_combine, identity)[1]
    weights = (
        jnp.einsum("hik,hjk->hij", query_rotated, key_rotated, precision=TOP_PRECISION) * decay_mask
    )
    retained_output = jnp.einsum("hij,hjv->hiv", weights, value_per_head, precision=TOP_PRECISION)
    retained_output = retained_output + per_head_decay[..., None] * jnp.einsum(
        "dzr,drs->dzs", query_rotated, incoming_state, precision=TOP_PRECISION
    )
    inverse_rms = lax.rsqrt(
        jnp.mean(retained_output * retained_output, axis=-1, keepdims=True) + EPSILON
    )
    normed = retained_output * inverse_rms
    normed_bf = (
        normed.transpose(1, 0, 2)
        .reshape(tokens_here, heads_local * value_width)
        .astype(jnp.bfloat16)
    )
    proj_grad = summed_rows(
        lax.dot_general(
            resid_grad, normed_bf, (((0,), (0,)), ((), ())), preferred_element_type=jnp.float32
        ),
        SP,
    )
    normed_grad = jnp.dot(resid_grad, out_proj, preferred_element_type=jnp.float32)
    normed_grad = normed_grad.reshape(tokens_here, heads_local, value_width).transpose(1, 0, 2)
    retention_gradient = inverse_rms * (
        normed_grad - normed * jnp.mean(normed_grad * normed, axis=-1, keepdims=True)
    )
    inner_gradient = jnp.einsum(
        "gwn,gwj->gnj",
        query_rotated * per_head_decay[..., None],
        retention_gradient,
        precision=TOP_PRECISION,
    )
    future_gradient = prefix_by_axis_2((carried, inner_gradient), SP, decay_combine, identity)[1]
    score_grad = (
        jnp.einsum("hiv,hjv->hij", retention_gradient, value_per_head, precision=TOP_PRECISION)
        * decay_mask
    )
    query_portion = jnp.einsum("hij,hjk->hik", score_grad, key_rotated, precision=TOP_PRECISION)
    query_portion = query_portion + per_head_decay[..., None] * jnp.einsum(
        "bpl,btl->bpt", retention_gradient, incoming_state, precision=TOP_PRECISION
    )
    key_portion = jnp.einsum("hij,hik->hjk", score_grad, query_rotated, precision=TOP_PRECISION)
    key_portion = key_portion + remaining_decay[..., None] * jnp.einsum(
        "uxn,ubn->uxb", value_per_head, future_gradient, precision=TOP_PRECISION
    )
    value_portion = jnp.einsum("hij,hiv->hjv", weights, retention_gradient, precision=TOP_PRECISION)
    value_portion = value_portion + remaining_decay[..., None] * jnp.einsum(
        "bui,bim->bum", key_rotated, future_gradient, precision=TOP_PRECISION
    )
    query_grad = turn(query_portion.transpose(1, 0, 2), cosines, -sines).astype(jnp.bfloat16)
    key_grad = (turn(key_portion.transpose(1, 0, 2), cosines, -sines) * key_scale).astype(
        jnp.bfloat16
    )
    value_grad = value_portion.transpose(1, 0, 2).astype(jnp.bfloat16)
    return (
        gate_part[None],
        up_part[None],
        down_part[None],
        proj_grad,
        query_grad,
        key_grad,
        value_grad,
    )


def solution(mesh):
    split = Mesh(mesh.devices.reshape(8, 4, 2, mesh.shape["tp"]), ("sp_0", "sp_1", "sp_2", "tp"))
    placed = (
        P(SP, None),
        P(SP, None),
        P(SP, None),
        P(SP, None),
        P(SP, "tp", None),
        P(SP, "tp", None),
        P(SP, "tp", None),
        P(SP, "tp"),
        P(None, "tp"),
        P(SP, None, "tp"),
        P(SP, None, "tp"),
        P(SP, "tp", None),
    )
    return jax.shard_map(
        per_device,
        mesh=split,
        in_specs=placed,
        out_specs=(
            P(SP, None, "tp"),
            P(SP, None, "tp"),
            P(SP, "tp", None),
            P(SP, "tp"),
            P(SP, "tp", None),
            P(SP, "tp", None),
            P(SP, "tp", None),
        ),
        check_vma=False,
    )
```

profile of v0, /device:TPU:33, one launch (start us, length us, event | category | flops | bytes accessed | tf_op | source)
XLA Modules:
  0.0 401.4 jit_solution(11609621116955901032)
XLA Ops:
  10.3 1.4 scatter_custom_fusion
  12.0 3.4 mul.753
  15.4 3.7 mul.754
  19.5 3.3 gather_fusion
  22.8 1.8 multiply_convert_fusion
  24.6 3.3 gather_fusion.1
  27.9 2.5 fusion.4
  30.4 2.3 pad_maximum_fusion
  32.7 12.4 %all-to-all-start = ((bf16[64,16,2048]{2,1,0:T(8,128)(2,1)}), bf16[64,16,2048]{2,1,0:T(8,128)(2,1)}, u32[]{:S(2)}, u32[]{:S(2)}) async-start(bf16[64,16,2048]{2,1,0:T(8,128)(2,1)} %pad_maximum_fusion), calls=%async_computation | async-start | bytes 8388608 | tf_op jit(solution)/shard_map/all_to_all | solution.py:19
  47.2 2.5 all-reduce
  49.8 9.4 %all-gather.3 = bf16[4,1,2]{2,1,0:T(2,128)(2,1)S(1)} all-gather(bf16[1,1,2]{2,1,0:T(2,128)(2,1)S(1)} %convert_bitcast_fusion.12), channel_id=1, replica_groups=mesh['sp_0'=8,'sp_1'=4,'sp_2'=2,'tp'=4] {'sp_1'}, dimensions={0}, use_global_device_ids=true | all-gather | bytes 20 | tf_op jit(solution)/shard_map/all_gather | solution.py:68
  63.0 3.4 all-gather
  66.4 73.2 %all-to-all-done = bf16[64,16,2048]{2,1,0:T(8,128)(2,1)} async-done(((bf16[64,16,2048]{2,1,0:T(8,128)(2,1)}), bf16[64,16,2048]{2,1,0:T(8,128)(2,1)}, u32[]{:S(2)}, u32[]{:S(2)}) %all-to-all-start) | async-done | bytes 4194336 | tf_op jit(solution)/shard_map/all_to_all | solution.py:19
  139.6 2.7 fusion.6
  142.3 2.5 fusion.7
  144.9 2.8 select_convert_fusion
  149.9 1.5 copy.218
  151.5 4.4 %all-to-all-start.1 = ((bf16[4,64,8,512]{3,2,1,0:T(8,128)(2,1)}), bf16[4,64,8,512]{3,2,1,0:T(8,128)(2,1)}, u32[]{:S(2)}, u32[]{:S(2)}) async-start(bf16[4,64,8,512]{3,2,1,0:T(8,128)(2,1)} %bitcast.511), calls=%async_computation.1 | async-start | bytes 4194304 | tf_op jit(solution)/shard_map/all_to_all | solution.py:36
  157.3 12.1 %all_gather.51 = bf16[4,2,128,256]{3,2,1,0:T(8,128)(2,1)S(1)} all-gather(bf16[1,2,128,256]{3,2,1,0:T(8,128)(2,1)S(1)} %fusion.64), channel_id=1, replica_groups=mesh['sp_0'=8,'sp_1'=4,'sp_2'=2,'tp'=4] {'sp_1'}, dimensions={0}, use_global_device_ids=true | all-gather | bytes 655360 | tf_op jit(solution)/shard_map/all_gather | solution.py:68
  171.3 13.0 %all-gather.4 = bf16[8,1,2]{2,1,0:T(2,128)(2,1)S(1)} all-gather(bf16[1,1,2]{2,1,0:T(2,128)(2,1)S(1)} %get-tuple-element.85), channel_id=1, replica_groups=mesh['sp_0'=8,'sp_1'=4,'sp_2'=2,'tp'=4] {'sp_0'}, dimensions={0}, use_global_device_ids=true | all-gather | bytes 36 | tf_op jit(solution)/shard_map/all_gather | solution.py:68
  184.5 2.9 reduce_sum.46
  187.4 10.3 %all-to-all-start.2 = ((bf16[64,8,512]{2,1,0:T(8,128)(2,1)}), bf16[64,8,512]{2,1,0:T(8,128)(2,1)S(1)}, u32[]{:S(2)}, u32[]{:S(2)}) async-start(bf16[64,8,512]{2,1,0:T(8,128)(2,1)} %reduce_sum.46), calls=%async_computation.2 | async-start | bytes 1048576 | tf_op jit(solution)/shard_map/all_to_all | solution.py:227
  199.0 1.2 compare_and_fusion
  200.8 1.5 subtract_exponential_fusion
  202.3 14.3 %all-to-all-done.2 = bf16[64,8,512]{2,1,0:T(8,128)(2,1)S(1)} async-done(((bf16[64,8,512]{2,1,0:T(8,128)(2,1)}), bf16[64,8,512]{2,1,0:T(8,128)(2,1)S(1)}, u32[]{:S(2)}, u32[]{:S(2)}) %all-to-all-start.2) | async-done | bytes 524320 | tf_op jit(solution)/shard_map/all_to_all | solution.py:227
  216.6 1.5 broadcast_in_dim.177
  218.2 4.6 %all-to-all-start.3 = ((bf16[4,64,8,512]{3,2,1,0:T(8,128)(2,1)}), bf16[4,64,8,512]{3,2,1,0:T(8,128)(2,1)}, u32[]{:S(2)}, u32[]{:S(2)}) async-start(bf16[4,64,8,512]{3,2,1,0:T(8,128)(2,1)} %broadcast_in_dim.177), calls=%async_computation.3 | async-start | bytes 4194304 | tf_op jit(solution)/shard_map/all_to_all | solution.py:42
  225.5 2.0 fusion.34
  227.9 1.6 multiply_reduce_fusion
  231.6 17.2 %all-to-all-done.3 = bf16[4,64,8,512]{3,2,1,0:T(8,128)(2,1)} async-done(((bf16[4,64,8,512]{3,2,1,0:T(8,128)(2,1)}), bf16[4,64,8,512]{3,2,1,0:T(8,128)(2,1)}, u32[]{:S(2)}, u32[]{:S(2)}) %all-to-all-start.3) | async-done | bytes 2097184 | tf_op jit(solution)/shard_map/all_to_all | solution.py:42
  248.8 3.3 copy.165
  252.1 4.4 %gather_fusion.2 = bf16[256,2048]{1,0:T(8,128)(2,1)S(1)} fusion(bf16[512,2048]{1,0:T(8,128)(2,1)} %bitcast.510, s32[1024]{0:T(1024)} %pad_clamp_fusion), kind=kCustom, calls=%fused_computation.2 | custom fusion | bytes 2098176 | tf_op jit(solution)/shard_map/jit(_take)/gather | solution.py:233
  256.5 1.5 gather.23
  258.0 2.0 fusion.24
  260.9 2.7 fusion.162
  264.3 10.6 %all-gather.5 = bf16[8,1,2]{2,1,0:T(2,128)(2,1)S(1)} all-gather(bf16[1,1,2]{2,1,0:T(2,128)(2,1)S(1)} %copy-done.49), channel_id=1, replica_groups=mesh['sp_0'=8,'sp_1'=4,'sp_2'=2,'tp'=4] {'sp_0'}, dimensions={0}, use_global_device_ids=true | all-gather | bytes 36 | tf_op jit(solution)/shard_map/all_gather | solution.py:95
  276.7 1.6 fusion.163
  280.3 6.4 %all-gather.2 = bf16[4,128,256]{2,1,0:T(8,128)(2,1)S(1)} all-gather(bf16[2,128,256]{2,1,0:T(8,128)(2,1)S(1)} %convolution_convert_fusion.3), channel_id=4, replica_groups=mesh['sp_0'=8,'sp_1'=4,'sp_2'=2,'tp'=4] {'sp_2'}, dimensions={0}, use_global_device_ids=true | all-gather | bytes 393216 | tf_op jit(solution)/shard_map/all_gather | solution.py:95
  287.4 10.0 %all_gather.57 = bf16[4,2,128,256]{3,2,1,0:T(8,128)(2,1)S(1)} all-gather(bf16[1,2,128,256]{3,2,1,0:T(8,128)(2,1)S(1)} %fusion.68), channel_id=1, replica_groups=mesh['sp_0'=8,'sp_1'=4,'sp_2'=2,'tp'=4] {'sp_1'}, dimensions={0}, use_global_device_ids=true | all-gather | bytes 655360 | tf_op jit(solution)/shard_map/all_gather | solution.py:95
  297.5 1.5 fusion.52
  299.0 3.4 fusion
  302.4 3.5 fusion.1
  305.9 3.5 fusion.2
  313.4 1.9 convolution_bitcast_fusion.4
  315.3 33.1 %all-gather.11.cloned.1.call-done = bf16[8,2,128,256]{3,2,1,0:T(8,128)(2,1)} async-done(((bf16[1,2,128,256]{3,2,1,0:T(8,128)(2,1)}), bf16[8,2,128,256]{3,2,1,0:T(8,128)(2,1)}) %all-gather.11.cloned.1.call-update) | async-done | bytes 1048592 | tf_op jit(solution)/shard_map/all_gather | solution.py:95
  348.5 2.0 fusion.31
  353.0 23.5 %reduce-scatter.6.cloned.1.call-done = f32[64,512]{1,0:T(8,128)} async-done(((f32[256,512]{1,0:T(8,128)}), f32[64,512]{1,0:T(8,128)}) %reduce-scatter.6.cloned.1.call-update) | async-done | bytes 131088 | tf_op jit(solution)/shard_map/reduce_scatter | solution.py:85
  379.4 15.5 %reduce-scatter.8.cloned.1.call-done = f32[32,512]{1,0:T(8,128)} async-done(((f32[64,512]{1,0:T(8,128)}), f32[32,512]{1,0:T(8,128)}) %reduce-scatter.8.cloned.1.call-update) | async-done | bytes 65552 | tf_op jit(solution)/shard_map/reduce_scatter | solution.py:85
  (218 shorter events, 36.8 us)
Async XLA Ops:
  7.2 269.5 %copy-start = (bf16[2048,512]{1,0:T(8,128)(2,1)S(1)}, bf16[2048,512]{1,0:T(8,128)(2,1)}, u32[]{:S(2)}) copy-start(bf16[2048,512]{1,0:T(8,128)(2,1)} %param.20) | copy-start | bytes 6291460
  15.4 3.7 copy-start.50
  15.4 4.1 %copy-start.1 = (bf16[128,2048]{1,0:T(8,128)(2,1)S(1)}, bf16[128,2048]{1,0:T(8,128)(2,1)}, u32[]{:S(2)}) copy-start(bf16[128,2048]{1,0:T(8,128)(2,1)} %param.12) | copy-start | bytes 1572868
  32.7 12.4 %copy-start.51 = (f32[128,2]{0,1:T(2,128)S(1)}, f32[128,2]{0,1:T(2,128)}, u32[]{:S(2)}) copy-start(f32[128,2]{0,1:T(2,128)} %param.19) | copy-start | bytes 3076
  32.7 12.8 %copy-start.53 = (u32[256]{0:T(256)S(1)}, u32[256]{0:T(256)}, u32[]{:S(2)}) copy-start(u32[256]{0:T(256)} %constant.149) | copy-start | bytes 3076
  32.7 26.4 %copy-start.28 = (bf16[128,2,128]{2,1,0:T(2,128)(2,1)S(1)}, bf16[128,2,128]{2,1,0:T(2,128)(2,1)}, u32[]{:S(2)}) copy-start(bf16[128,2,128]{2,1,0:T(2,128)(2,1)} %param.16) | copy-start | bytes 196612
  32.7 26.6 %copy-start.29 = (bf16[128,2,128]{2,1,0:T(2,128)(2,1)S(1)}, bf16[128,2,128]{2,1,0:T(2,128)(2,1)}, u32[]{:S(2)}) copy-start(bf16[128,2,128]{2,1,0:T(2,128)(2,1)} %param.17) | copy-start | bytes 196612
  32.7 106.9 %all-to-all-start = ((bf16[64,16,2048]{2,1,0:T(8,128)(2,1)}), bf16[64,16,2048]{2,1,0:T(8,128)(2,1)}, u32[]{:S(2)}, u32[]{:S(2)}) async-start(bf16[64,16,2048]{2,1,0:T(8,128)(2,1)} %pad_maximum_fusion), calls=%async_computation | async-start | bytes 8388608 | tf_op jit(solution)/shard_map/all_to_all | solution.py:19
  45.1 17.5 %copy-start.6 = (bf16[128,2,256]{2,1,0:T(2,128)(2,1)S(1)}, bf16[128,2,256]{2,1,0:T(2,128)(2,1)}, u32[]{:S(2)}) copy-start(bf16[128,2,256]{2,1,0:T(2,128)(2,1)} %param.18) | copy-start | bytes 393220
  45.4 15.4 %copy-start.18 = (f32[128,2]{1,0:T(8,128)}, f32[128,2]{1,0:T(8,128)S(1)}, u32[]{:S(2)}) copy-start(f32[128,2]{1,0:T(8,128)S(1)} %reduce_window_sum.28) | copy-start | bytes 3076
  45.5 17.1 %copy-start.30 = (f32[128,2]{0,1:T(2,128)}, f32[128,2]{0,1:T(2,128)S(1)}, u32[]{:S(2)}) copy-start(f32[128,2]{0,1:T(2,128)S(1)} %copy.172) | copy-start | bytes 3076
  61.7 80.6 %copy-start.11 = (f32[128,2,64,2]{0,3,2,1:T(2,128)}, f32[128,2,64,2]{0,3,2,1:T(2,128)S(1)}, u32[]{:S(2)}) copy-start(f32[128,2,64,2]{0,3,2,1:T(2,128)S(1)} %get-tuple-element.105) | copy-start | bytes 393220
  151.5 33.1 %all-to-all-start.1 = ((bf16[4,64,8,512]{3,2,1,0:T(8,128)(2,1)}), bf16[4,64,8,512]{3,2,1,0:T(8,128)(2,1)}, u32[]{:S(2)}, u32[]{:S(2)}) async-start(bf16[4,64,8,512]{3,2,1,0:T(8,128)(2,1)} %bitcast.511), calls=%async_computation.1 | async-start | bytes 4194304 | tf_op jit(solution)/shard_map/all_to_all | solution.py:36
  155.9 69.6 %all-gather.9.cloned.1.call-start = ((), (), s32[]{:S(2)}) async-start(), calls=%async_computation.7 | async-start | bytes 1179648 | tf_op jit(solution)/shard_map/all_gather | solution.py:68
  156.5 30.9 %copy-start.44 = (f32[2]{0:T(128)}, f32[2]{0:T(128)S(1)}, u32[]{:S(2)}) copy-start(f32[2]{0:T(128)S(1)} %get-tuple-element.102) | copy-start | bytes 28
  157.1 14.2 %copy-start.42 = (f32[2]{0:T(128)}, f32[2]{0:T(128)S(1)}, u32[]{:S(2)}) copy-start(f32[2]{0:T(128)S(1)} %get-tuple-element.83) | copy-start | bytes 28
  157.1 30.3 %copy-start.43 = (f32[2]{0:T(128)}, f32[2]{0:T(128)S(1)}, u32[]{:S(2)}) copy-start(f32[2]{0:T(128)S(1)} %get-tuple-element.99) | copy-start | bytes 28
  187.4 29.2 %all-to-all-start.2 = ((bf16[64,8,512]{2,1,0:T(8,128)(2,1)}), bf16[64,8,512]{2,1,0:T(8,128)(2,1)S(1)}, u32[]{:S(2)}, u32[]{:S(2)}) async-start(bf16[64,8,512]{2,1,0:T(8,128)(2,1)} %reduce_sum.46), calls=%async_computation.2 | async-start | bytes 1048576 | tf_op jit(solution)/shard_map/all_to_all | solution.py:227
  218.2 4.9 %copy-start.47 = (s32[256,1]{0,1:T(1,128)S(1)}, s32[256,1]{0,1:T(1,128)}, u32[]{:S(2)}) copy-start(s32[256,1]{0,1:T(1,128)} %copy-done.46) | copy-start | bytes 3076
  218.2 5.5 %copy-start.10 = (f32[128,2,64,2]{0,3,2,1:T(2,128)S(1)}, f32[128,2,64,2]{0,3,2,1:T(2,128)}, u32[]{:S(2)}) copy-start(f32[128,2,64,2]{0,3,2,1:T(2,128)} %get-tuple-element.104) | copy-start | bytes 393220
  218.2 5.6 %copy-start.24 = (f32[128,2]{1,0:T(8,128)S(1)}, f32[128,2]{1,0:T(8,128)}, u32[]{:S(2)}) copy-start(f32[128,2]{1,0:T(8,128)} %get-tuple-element.63) | copy-start | bytes 3076
  218.2 6.2 %copy-start.31 = (f32[128,2]{0,1:T(2,128)S(1)}, f32[128,2]{0,1:T(2,128)}, u32[]{:S(2)}) copy-start(f32[128,2]{0,1:T(2,128)} %copy-done.30) | copy-start | bytes 3076
  218.2 30.6 %all-to-all-start.3 = ((bf16[4,64,8,512]{3,2,1,0:T(8,128)(2,1)}), bf16[4,64,8,512]{3,2,1,0:T(8,128)(2,1)}, u32[]{:S(2)}, u32[]{:S(2)}) async-start(bf16[4,64,8,512]{3,2,1,0:T(8,128)(2,1)} %broadcast_in_dim.177), calls=%async_computation.3 | async-start | bytes 4194304 | tf_op jit(solution)/shard_map/all_to_all | solution.py:42
  222.8 5.0 %copy-start.7 = (bf16[128,2,256]{2,1,0:T(2,128)(2,1)S(1)}, bf16[128,2,256]{2,1,0:T(2,128)(2,1)}, u32[]{:S(2)}) copy-start(bf16[128,2,256]{2,1,0:T(2,128)(2,1)} %param.18) | copy-start | bytes 393220
  222.8 90.3 %reduce-scatter.4.cloned.1.call-start = ((), (), s32[]{:S(2)}) async-start(), calls=%async_computation.8 | async-start | bytes 4718592 | tf_op jit(solution)/shard_map/reduce_scatter | solution.py:85
  223.8 5.7 %copy-start.3 = (f32[128,2,128]{2,0,1:T(8,128)}, f32[128,2,128]{2,0,1:T(8,128)S(1)}, u32[]{:S(2)}) copy-start(f32[128,2,128]{2,0,1:T(8,128)S(1)} %copy.168) | copy-start | bytes 393220
  263.6 11.2 %copy-start.23 = (f32[128,2]{1,0:T(8,128)S(1)}, f32[128,2]{1,0:T(8,128)}, u32[]{:S(2)}) copy-start(f32[128,2]{1,0:T(8,128)} %get-tuple-element.62) | copy-start | bytes 3076
  263.7 15.7 %copy-start.2 = (f32[2,128,256]{2,1,0:T(8,128)S(1)}, f32[2,128,256]{2,1,0:T(8,128)}, u32[]{:S(2)}) copy-start(f32[2,128,256]{2,1,0:T(8,128)} %get-tuple-element.45) | copy-start | bytes 786436
  263.7 15.7 %copy-start.39 = (f32[2,128]{1,0:T(2,128)S(1)}, f32[2,128]{1,0:T(2,128)}, u32[]{:S(2)}) copy-start(f32[2,128]{1,0:T(2,128)} %get-tuple-element.95) | copy-start | bytes 3076
  263.7 84.8 %all-gather.11.cloned.1.call-start = ((), (), s32[]{:S(2)}) async-start(), calls=%async_computation.11 | async-start | bytes 1179648 | tf_op jit(solution)/shard_map/all_gather | solution.py:95
  276.7 3.1 copy-start.4
  276.7 3.1 copy-start.40
  298.9 77.5 %reduce-scatter.6.cloned.1.call-start = ((), (), s32[]{:S(2)}) async-start(), calls=%async_computation.9 | async-start | bytes 655360 | tf_op jit(solution)/shard_map/reduce_scatter | solution.py:85
  299.0 3.4 copy-start.27
  302.4 3.5 copy-start.55
  302.4 3.5 copy-start.57
  305.8 3.5 copy-start.8
  305.9 3.5 copy-start.32
  305.9 4.4 %copy-start.12 = (f32[128,2,64,2]{0,3,2,1:T(2,128)S(1)}, f32[128,2,64,2]{0,3,2,1:T(2,128)}, u32[]{:S(2)}) copy-start(f32[128,2,64,2]{0,3,2,1:T(2,128)} %copy-done.11) | copy-start | bytes 393220
  305.9 4.8 %copy-start.14 = (f32[2,128,128]{2,1,0:T(8,128)S(1)}, f32[2,128,128]{2,1,0:T(8,128)}, u32[]{:S(2)}) copy-start(f32[2,128,128]{2,1,0:T(8,128)} %convolution_multiply_fusion.1) | copy-start | bytes 393220
  305.9 6.0 %copy-start.37 = (f32[128,2]{0,1:T(2,128)S(1)}, f32[128,2]{0,1:T(2,128)}, u32[]{:S(2)}) copy-start(f32[128,2]{0,1:T(2,128)} %copy.174) | copy-start | bytes 3076
  309.7 38.8 %copy-start.34 = (f32[2]{0:T(128)S(1)}, f32[2]{0:T(128)}, u32[]{:S(2)}) copy-start(f32[2]{0:T(128)} %copy-done.33) | copy-start | bytes 28
  309.7 38.8 %copy-start.36 = (f32[2]{0:T(128)S(1)}, f32[2]{0:T(128)}, u32[]{:S(2)}) copy-start(f32[2]{0:T(128)} %copy-done.35) | copy-start | bytes 28
  309.7 38.8 %copy-start.41 = (f32[2]{0:T(128)S(1)}, f32[2]{0:T(128)}, u32[]{:S(2)}) copy-start(f32[2]{0:T(128)} %get-tuple-element.82) | copy-start | bytes 28
  310.7 39.8 %copy-start.38 = (f32[128,2]{0,1:T(2,128)S(1)}, f32[128,2]{0,1:T(2,128)}, u32[]{:S(2)}) copy-start(f32[128,2]{0,1:T(2,128)} %copy.184) | copy-start | bytes 3076
  313.1 81.7 %reduce-scatter.8.cloned.1.call-start = ((), (), s32[]{:S(2)}) async-start(), calls=%async_computation.10 | async-start | bytes 196608 | tf_op jit(solution)/shard_map/reduce_scatter | solution.py:85
  315.3 62.9 %copy-start.15 = (f32[128,2,256]{2,0,1:T(8,128)S(1)}, f32[128,2,256]{2,0,1:T(8,128)}, u32[]{:S(2)}) copy-start(f32[128,2,256]{2,0,1:T(8,128)} %convolution_bitcast_fusion.1) | copy-start | bytes 786436
  348.5 3.2 copy-start.21
  (19 other events, 29.9 us)
Sparse Core Ops, SparseCore 0:
  170.9 34.8 all-gather.8
  263.8 49.2 reduce-scatter.3
  314.9 33.5 all-gather.10
  350.8 25.6 reduce-scatter.5
  379.4 15.4 reduce-scatter.7
where the time goes:
time: 404 us; the launch traced here: 401 us
  waiting for transfers between devices  177 us (44%)
  blocking collectives  67.4 us (17%)
  local copies, waits for them, and re-layouts  39.3 us (10%)
  other arithmetic  35.3 us (9%)
  matrix products  34.4 us (9%)
  starting transfers between devices  32.4 us (8%)
  between operations  15.3 us (4%)
    all_to_all x1, waiting for transfers between devices, in_one_piece(): lax.all_to_all(both, axis, split_axis=split_dim, concat_axis=concat_dim,...  73.2 us
    reduce_scatter x3, waiting for transfers between devices, summed_rows(): total = lax.psum_scatter(total, axis, scatter_dimension=0, tiled=True)  39.3 us
    all_gather x4, blocking collectives, prefix_by_axis(): lax.all_gather(part.astype(kind), axis)  37.9 us
    all_gather x1, waiting for transfers between devices, prefix_by_axis_2(): lax.all_gather(part.astype(kind), axis)  33.1 us
    all_gather x3, blocking collectives, prefix_by_axis_2(): lax.all_gather(part.astype(kind), axis)  27 us
    all_to_all x1, waiting for transfers between devices, copy_for_each(): return lax.all_to_all(copies, axis, split_axis=0, concat_axis=0, tiled=True)  17.2 us
    all_to_all x1, waiting for transfers between devices, per_device(): lax.all_to_all(shares.astype(jnp.bfloat16), SP, split_axis=0, concat_axis...  14.3 us
    all_to_all x1, starting transfers between devices, in_one_piece(): lax.all_to_all(both, axis, split_axis=split_dim, concat_axis=concat_dim,...  12.4 us
  transfers between devices with their start and end apart: 9, of which 7 were waited for; matrix products, arithmetic and copies ran while one was open for 14% of the time, Pallas kernels for 0%

commit v1 on v0

--- a/solution.py
+++ b/solution.py
@@ -1,6 +1,8 @@
 import jax
 import jax.numpy as jnp
 from jax import lax
+from jax.experimental import pallas as pl
+from jax.experimental.pallas import tpu as pltpu
 from jax.sharding import Mesh
 from jax.sharding import PartitionSpec as P
 
@@ -140,44 +142,329 @@
     return (earlier[0] * next_rows[0], next_rows[1] + next_rows[0][:, None, None] * earlier[1])
 
 
-def expert_local(routed_rows, routed_grads, gate_w, up_w, down_w):
-    gate_pre = jnp.dot(routed_rows, gate_w, preferred_element_type=jnp.float32)
-    up_pre = jnp.dot(routed_rows, up_w, preferred_element_type=jnp.float32)
-    gate_clip = jnp.minimum(gate_pre, CLAMP_LIMIT)
-    up_clip = jnp.clip(up_pre, -CLAMP_LIMIT, CLAMP_LIMIT)
-    sigmoid_gate = jax.nn.sigmoid(GATE_SLOPE * gate_clip)
-    activated = (gate_clip * sigmoid_gate * (up_clip + 1.0)).astype(jnp.bfloat16)
-    down_part = lax.dot_general(
-        activated, routed_grads, (((0,), (0,)), ((), ())), preferred_element_type=jnp.float32
-    )
-    act_grad = lax.dot_general(
-        routed_grads, down_w, (((1,), (1,)), ((), ())), preferred_element_type=jnp.float32
-    )
-    slope = sigmoid_gate + GATE_SLOPE * gate_clip * sigmoid_gate * (1.0 - sigmoid_gate)
-    gate_pre_grad = jnp.where(
-        gate_pre < CLAMP_LIMIT, act_grad * (up_clip + 1.0) * slope, 0.0
-    ).astype(jnp.bfloat16)
-    up_pre_grad = jnp.where(
-        jnp.abs(up_pre) < CLAMP_LIMIT, act_grad * gate_clip * sigmoid_gate, 0.0
-    ).astype(jnp.bfloat16)
-    gate_part = lax.dot_general(
-        routed_rows, gate_pre_grad, (((0,), (0,)), ((), ())), preferred_element_type=jnp.float32
-    )
-    up_part = lax.dot_general(
-        routed_rows, up_pre_grad, (((0,), (0,)), ((), ())), preferred_element_type=jnp.float32
-    )
-    back_rows = lax.dot_general(
-        gate_pre_grad, gate_w, (((1,), (1,)), ((), ())), preferred_element_type=jnp.float32
-    )
-    back_rows = back_rows + lax.dot_general(
-        up_pre_grad, up_w, (((1,), (1,)), ((), ())), preferred_element_type=jnp.float32
-    )
-    return (
-        gate_part.astype(jnp.bfloat16),
-        up_part.astype(jnp.bfloat16),
-        down_part.astype(jnp.bfloat16),
-        back_rows.astype(jnp.bfloat16),
-    )
+MESH = pl.DeviceIdType.MESH
+BF = jnp.bfloat16
+F32 = jnp.float32
+
+
+def dot(a, b, ca, cb, precision=None):
+    return lax.dot_general(
+        a, b, (((ca,), (cb,)), ((), ())), preferred_element_type=F32, precision=precision
+    )
+
+
+def place_of(p, x):
+    return (p // 8, p // 2 % 4, p % 2, x)
+
+
+def remote(src, dst, send_sem, recv_sem, device):
+    pltpu.make_async_remote_copy(
+        src_ref=src,
+        dst_ref=dst,
+        send_sem=send_sem,
+        recv_sem=recv_sem,
+        device_id=place_of(*device),
+        device_id_type=MESH,
+    ).start()
+
+
+def take(ref, sem):
+    pltpu.make_async_copy(ref, ref, sem).wait()
+
+
+def expert_kernel(
+    stream,
+    og,
+    routes,
+    weight,
+    gate_w,
+    up_w,
+    down_w,
+    o_gate,
+    o_up,
+    o_down,
+    o_resid,
+    sq,
+    oq,
+    w,
+    d,
+    pm,
+    send,
+    rg,
+    gu,
+    ac,
+    bk,
+    xin,
+    acc,
+    fin,
+    ret,
+    rt,
+    lsem,
+    dsend,
+    drecv,
+    xsend,
+    xrecv,
+    rsend,
+    rrecv,
+    tsend,
+    trecv,
+    gsend,
+    grecv,
+):
+    me = lax.axis_index(SP)
+    x = lax.axis_index("tp")
+    z, j = me // 8, me % 8
+    right, left, far = (x + 1) % 4, (x + 3) % 4, (x + 2) % 4
+
+    barrier = pltpu.get_barrier_semaphore()
+
+    def hello(k, _):
+        pl.semaphore_signal(
+            barrier, inc=1, device_id=place_of((me + k) % 64, x), device_id_type=MESH
+        )
+        return 0
+
+    lax.fori_loop(1, 64, hello, 0)
+    for peer in (right, left, far):
+        pl.semaphore_signal(barrier, inc=1, device_id=place_of(me, peer), device_id_type=MESH)
+
+    cols = pl.ds(pl.multiple_of(x * 512, 512), 512)
+    loads = [
+        pltpu.make_async_copy(stream.at[:, cols], sq, lsem.at[0]),
+        pltpu.make_async_copy(og.at[:, cols], oq, lsem.at[1]),
+        pltpu.make_async_copy(gate_w.at[0], w.at[:, pl.ds(0, 256)], lsem.at[2]),
+        pltpu.make_async_copy(up_w.at[0], w.at[:, pl.ds(256, 256)], lsem.at[3]),
+        pltpu.make_async_copy(down_w.at[0], d, lsem.at[4]),
+    ]
+    for c in loads:
+        c.start()
+
+    ident = (
+        lax.broadcasted_iota(jnp.int32, (128, 128), 0)
+        == lax.broadcasted_iota(jnp.int32, (128, 128), 1)
+    ).astype(F32)
+    earlier = (
+        lax.broadcasted_iota(jnp.int32, (128, 128), 0)
+        < lax.broadcasted_iota(jnp.int32, (128, 128), 1)
+    ).astype(BF)
+    ids = dot(routes[...].astype(F32), ident, 0, 0)
+    wrow = dot(weight[...], ident, 0, 0, lax.Precision.HIGHEST)
+    expert = lax.broadcasted_iota(jnp.int32, (64, 128), 0).astype(F32)
+    named0 = (expert == ids[0:1]).astype(F32)
+    named1 = (expert == ids[1:2]).astype(F32)
+    before = dot((named0 + named1).astype(BF), earlier, 1, 0)
+    dest0 = ids[0:1] * 8.0 + jnp.sum(named0 * before, axis=0, keepdims=True)
+    dest1 = ids[1:2] * 8.0 + jnp.sum(named1 * before, axis=0, keepdims=True)
+    slot = lax.broadcasted_iota(jnp.int32, (512, 128), 0).astype(F32)
+    at0 = (slot == dest0).astype(F32)
+    at1 = (slot == dest1).astype(F32)
+    wslot = jnp.sum(at0 * wrow[0:1] + at1 * wrow[1:2], axis=1, keepdims=True)
+    place = (at0 + at1).astype(BF)
+    pm[...] = place
+    loads[0].wait()
+    send[:, 0:8, :] = dot(place, sq[...], 1, 0).reshape(64, 8, 512).astype(BF)
+    loads[1].wait()
+    send[:, 8:16, :] = (dot(place, oq[...], 1, 0) * wslot).reshape(64, 8, 512).astype(BF)
+
+    pl.semaphore_wait(barrier, 66)
+
+    order = (0, 1, 7, 2, 6, 3, 5, 4)
+
+    def plane(dz):
+        return (z + dz) % 8
+
+    def dispatch(dz):
+        def one(k, _):
+            p = plane(dz) * 8 + (j + k) % 8
+            remote(send.at[p], rg.at[x, me], dsend, drecv.at[dz], (p, x))
+            return 0
+
+        lax.fori_loop(1 if dz == 0 else 0, 8, one, 0)
+
+    for dz in order:
+        dispatch(dz)
+    rg[x, me] = send[me]
+
+    def group(q, dz):
+        return rg.at[q, pl.ds(plane(8 - dz) * 8, 8)]
+
+    def half(q, dz, h):
+        return rg.at[q, pl.ds(plane(8 - dz) * 8 + 4 * h, 4)]
+
+    def spread(dz):
+        if dz == 0:
+            take(rg.at[0, pl.ds(0, 7)], drecv.at[0])
+        else:
+            take(rg.at[0, pl.ds(0, 8)], drecv.at[dz])
+        remote(group(x, dz), group(x, dz), xsend, xrecv.at[0, dz], (me, right))
+        remote(group(x, dz), group(x, dz), xsend, xrecv.at[1, dz], (me, left))
+
+    def pass_on(dz):
+        take(group(left, dz), xrecv.at[0, dz])
+        remote(half(left, dz, 0), half(left, dz, 0), xsend, xrecv.at[2, dz], (me, right))
+        take(group(right, dz), xrecv.at[1, dz])
+        remote(half(right, dz, 1), half(right, dz, 1), xsend, xrecv.at[3, dz], (me, left))
+
+    spread(order[0])
+    for at, dz in enumerate(order):
+        if at + 1 < 8:
+            spread(order[at + 1])
+        pass_on(dz)
+    for dz in order:
+        take(half(far, dz, 0), xrecv.at[2, dz])
+        take(half(far, dz, 1), xrecv.at[3, dz])
+
+    for c in loads[2:]:
+        c.wait()
+
+    pairs = ((1, 7), (2, 6), (3, 5), (4, 0))
+
+    def experts(m):
+        za, zb = plane(pairs[m][0]), plane(pairs[m][1])
+
+        def both(q, part):
+            rows = pl.ds(8 * part, 8)
+            a = rg[q, pl.ds(za * 8, 8), rows, :].reshape(64, 512)
+            b = rg[q, pl.ds(zb * 8, 8), rows, :].reshape(64, 512)
+            return jnp.concatenate([a, b], axis=0)
+
+        pre = dot(both(0, 0), w[0:512, :], 1, 0)
+        back = dot(both(0, 1), d[:, 0:512], 1, 1)
+        for q in range(1, 4):
+            pre = pre + dot(both(q, 0), w[q * 512 : (q + 1) * 512, :], 1, 0)
+            back = back + dot(both(q, 1), d[:, q * 512 : (q + 1) * 512], 1, 1)
+        gate_pre, up_pre = pre[:, 0:256], pre[:, 256:512]
+        gate_clip = jnp.minimum(gate_pre, CLAMP_LIMIT)
+        up_clip = jnp.clip(up_pre, -CLAMP_LIMIT, CLAMP_LIMIT)
+        sig = jax.nn.sigmoid(GATE_SLOPE * gate_clip)
+        activated = (gate_clip * sig * (up_clip + 1.0)).astype(BF)
+        slope = sig + GATE_SLOPE * gate_clip * sig * (1.0 - sig)
+        gate_g = jnp.where(gate_pre < CLAMP_LIMIT, back * (up_clip + 1.0) * slope, 0.0).astype(BF)
+        up_g = jnp.where(jnp.abs(up_pre) < CLAMP_LIMIT, back * gate_clip * sig, 0.0).astype(BF)
+        both_g = jnp.concatenate([gate_g, up_g], axis=1)
+        for part, zz in ((0, za), (1, zb)):
+            at = pl.ds(pl.multiple_of(zz * 64, 64), 64)
+            gu[at, :] = both_g[64 * part : 64 * part + 64]
+            ac[at, :] = activated[64 * part : 64 * part + 64]
+        for q in range(4):
+            rows = dot(both_g, w[q * 512 : (q + 1) * 512, :], 1, 1).astype(BF)
+            bk[q, pl.ds(za * 8, 8)] = rows[0:64].reshape(8, 8, 512)
+            bk[q, pl.ds(zb * 8, 8)] = rows[64:128].reshape(8, 8, 512)
+
+        pa, pb = pl.ds(za * 8, 8), pl.ds(zb * 8, 8)
+        remote(bk.at[far, pa], xin.at[0, m], rsend, rrecv.at[0, m], (me, right))
+        remote(bk.at[far, pb], xin.at[1, m], rsend, rrecv.at[1, m], (me, left))
+        remote(bk.at[left, pa], xin.at[2, m], rsend, rrecv.at[2, m], (me, left))
+        remote(bk.at[right, pb], xin.at[3, m], rsend, rrecv.at[3, m], (me, right))
+
+    def forward(m):
+        pa, pb = (pl.ds(plane(dz) * 8, 8) for dz in pairs[m])
+        take(xin.at[0, m], rrecv.at[0, m])
+        acc[0, m] = (xin[0, m].astype(F32) + bk[right, pa].astype(F32)).astype(BF)
+        remote(acc.at[0, m], xin.at[4, m], rsend, rrecv.at[4, m], (me, right))
+        take(xin.at[1, m], rrecv.at[1, m])
+        acc[1, m] = (xin[1, m].astype(F32) + bk[left, pb].astype(F32)).astype(BF)
+        remote(acc.at[1, m], xin.at[5, m], rsend, rrecv.at[5, m], (me, left))
+
+    def finish(m):
+        for part, dz in enumerate(pairs[m]):
+            at = pl.ds(plane(dz) * 8, 8)
+            direct, summed = 2 + part, 4 + part
+            take(xin.at[direct, m], rrecv.at[direct, m])
+            take(xin.at[summed, m], rrecv.at[summed, m])
+            fin[at] = (
+                bk[x, at].astype(F32) + xin[direct, m].astype(F32) + xin[summed, m].astype(F32)
+            ).astype(BF)
+
+            def one(k, _, dz=dz):
+                p = plane(dz) * 8 + (j + k) % 8
+                remote(fin.at[p], ret.at[me], tsend, trecv, (p, x))
+                return 0
+
+            lax.fori_loop(1 if dz == 0 else 0, 8, one, 0)
+            if dz == 0:
+                ret[me] = fin[me]
+
+    def weight_grads(q):
+        at = pl.ds(q * 512, 512)
+        rows = rg[q, :, 0:8, :].reshape(512, 512)
+        grads = rg[q, :, 8:16, :].reshape(512, 512)
+        both = dot(rows, gu[...], 0, 0).astype(BF)
+        o_gate[at, :] = both[:, 0:256]
+        o_up[at, :] = both[:, 256:512]
+        o_down[:, at] = dot(ac[...], grads, 0, 0).astype(BF)
+
+    for m in range(4):
+        experts(m)
+        if m >= 1:
+            forward(m - 1)
+    forward(3)
+    for m in range(4):
+        finish(m)
+        weight_grads(m)
+
+    take(ret.at[pl.ds(0, 63)], trecv)
+    resid = dot(ret[...].reshape(512, 512), pm[...], 0, 0) + dot(oq[...], ident.astype(BF), 0, 0)
+    rt[x] = resid.astype(BF)
+    for k, peer in enumerate((right, left, far)):
+        remote(rt.at[x], rt.at[x], gsend, grecv.at[k], (me, peer))
+    for k, peer in enumerate((left, right, far)):
+        take(rt.at[peer], grecv.at[k])
+    o_resid[...] = rt[...].reshape(2048, 128)
+
+    take(send.at[pl.ds(0, 63)], dsend)
+    take(rg.at[pl.ds(0, 3)], xsend)
+    take(xin, rsend)
+    take(fin.at[pl.ds(0, 63)], tsend)
+    take(rt.at[pl.ds(0, 3)], gsend)
+
+
+def expert_call(stream, out_grad, routes, route_weight, gate_weight, up_weight, down_weight):
+    anywhere = pl.BlockSpec(memory_space=pl.ANY)
+    local = pl.BlockSpec(memory_space=pltpu.VMEM)
+    dma = pltpu.SemaphoreType.DMA
+    return pl.pallas_call(
+        expert_kernel,
+        out_shape=(
+            jax.ShapeDtypeStruct((2048, 256), BF),
+            jax.ShapeDtypeStruct((2048, 256), BF),
+            jax.ShapeDtypeStruct((256, 2048), BF),
+            jax.ShapeDtypeStruct((2048, 128), BF),
+        ),
+        in_specs=[anywhere, anywhere, local, local, anywhere, anywhere, anywhere],
+        out_specs=(local, local, local, local),
+        scratch_shapes=[
+            pltpu.VMEM((128, 512), BF),
+            pltpu.VMEM((128, 512), BF),
+            pltpu.VMEM((2048, 512), BF),
+            pltpu.VMEM((256, 2048), BF),
+            pltpu.VMEM((512, 128), BF),
+            pltpu.VMEM((64, 16, 512), BF),
+            pltpu.VMEM((4, 64, 16, 512), BF),
+            pltpu.VMEM((512, 512), BF),
+            pltpu.VMEM((512, 256), BF),
+            pltpu.VMEM((4, 64, 8, 512), BF),
+            pltpu.VMEM((6, 4, 8, 8, 512), BF),
+            pltpu.VMEM((2, 4, 8, 8, 512), BF),
+            pltpu.VMEM((64, 8, 512), BF),
+            pltpu.VMEM((64, 8, 512), BF),
+            pltpu.VMEM((4, 512, 128), BF),
+            dma((5,)),
+            dma,
+            dma((8,)),
+            dma,
+            dma((4, 8)),
+            dma,
+            dma((6, 4)),
+            dma,
+            dma,
+            dma,
+            dma((3,)),
+        ],
+        compiler_params=pltpu.CompilerParams(
+            collective_id=0, has_side_effects=True, vmem_limit_bytes=60 * 1024 * 1024
+        ),
+    )(stream, out_grad, routes, route_weight, gate_weight, up_weight, down_weight)
 
 
 def per_device(
@@ -194,48 +481,9 @@
     up_weight,
     down_weight,
 ):
-    experts = lax.axis_size(SP)
     tokens_here = stream.shape[0]
-    model_width = stream.shape[1]
-    capacity = 4 * tokens_here // experts
-    pair_count = 2 * tokens_here
-    flat_ids, slot_ids = slot_numbers(routes, experts)
-    destination = flat_ids * capacity + slot_ids
-    source = (
-        jnp.full((experts * capacity,), -1, jnp.int32)
-        .at[destination]
-        .set(jnp.arange(pair_count, dtype=jnp.int32))
-    )
-    present = (source >= 0)[:, None]
-    picked = jnp.maximum(source, 0)
-    zero_value = jnp.zeros((), jnp.bfloat16)
-    pair_grad = (route_weight[:, :, None] * out_grad[:, None, :].astype(jnp.float32)).astype(
-        jnp.bfloat16
-    )
-    pair_grad = pair_grad.reshape(pair_count, model_width)
-    send_rows = jnp.where(present, jnp.take(stream, picked // 2, axis=0), zero_value)
-    send_rows = send_rows.reshape(experts, capacity, model_width)
-    send_grads = jnp.where(present, jnp.take(pair_grad, picked, axis=0), zero_value)
-    send_grads = send_grads.reshape(experts, capacity, model_width)
-    routed_rows, routed_grads = in_one_piece((send_rows, send_grads), SP, 0, 0, 1)
-    routed_rows = routed_rows.reshape(experts * capacity, model_width)
-    routed_grads = routed_grads.reshape(experts * capacity, model_width)
-    gate_part, up_part, down_part, back_rows = expert_local(
-        routed_rows, routed_grads, gate_weight[0], up_weight[0], down_weight[0]
-    )
-    shares = sent_and_summed(back_rows.reshape(experts, capacity, model_width), "tp", 2)
-    shares = lax.all_to_all(
-        shares.astype(jnp.bfloat16), SP, split_axis=0, concat_axis=0, tiled=True
-    )
-    returned = collect(shares, "tp", 2)
-    returned = returned.reshape(experts * capacity, model_width)
-    per_pair = (
-        jnp.take(returned, destination, axis=0)
-        .reshape(tokens_here, 2, model_width)
-        .astype(jnp.float32)
-    )
-    resid_grad = (out_grad.astype(jnp.float32) + per_pair[:, 0] + per_pair[:, 1]).astype(
-        jnp.bfloat16
+    gate_part, up_part, down_part, resid_t = expert_call(
+        stream, out_grad, routes, route_weight, gate_weight, up_weight, down_weight
     )
     heads_local = queries.shape[1]
     key_width = queries.shape[2]
@@ -281,11 +529,13 @@
     )
     proj_grad = summed_rows(
         lax.dot_general(
-            resid_grad, normed_bf, (((0,), (0,)), ((), ())), preferred_element_type=jnp.float32
+            resid_t, normed_bf, (((1,), (0,)), ((), ())), preferred_element_type=jnp.float32
         ),
         SP,
     )
-    normed_grad = jnp.dot(resid_grad, out_proj, preferred_element_type=jnp.float32)
+    normed_grad = lax.dot_general(
+        resid_t, out_proj, (((0,), (0,)), ((), ())), preferred_element_type=jnp.float32
+    )
     normed_grad = normed_grad.reshape(tokens_here, heads_local, value_width).transpose(1, 0, 2)
     retention_gradient = inverse_rms * (
         normed_grad - normed * jnp.mean(normed_grad * normed, axis=-1, keepdims=True)

time: 404 us -> 322 us (0.80)
  Pallas kernels: 0 us -> 101 us
  waiting for transfers between devices: 177 us -> 79.3 us
  starting transfers between devices: 32.4 us -> 0.42 us
  local copies, waits for them, and re-layouts: 39.3 us -> 19.3 us
  matrix products: 34.4 us -> 19.1 us
  other arithmetic: 35.3 us -> 20.9 us
    all_to_all x4 -> x0, waiting for transfers between devices: 105 us -> none  [the longest x1 73.2 us: in_one_piece(): lax.all_to_all(both, axis, split_axis=split_dim, concat_axis=concat_dim,...]
    pallas_call x0 -> x1, Pallas kernels: none -> 101 us  [expert_call(): pl.pallas_call(expert_kernel, out_shape=(jax.ShapeDtypeStruct((2048, 256)...]
    all_to_all x4 -> x0, starting transfers between devices: 31.7 us -> none  [the longest x1 12.4 us: in_one_piece(): lax.all_to_all(both, axis, split_axis=split_dim, concat_axis=concat_dim,...]
    dot_general x10 -> x2, matrix products: 24.2 us -> 5.35 us  [the longest x1 3.71 us: per_device(): lax.dot_general(resid_t, normed_bf, (((1,), (0,)), ((), ())), preferred_e...]
    gather x4 -> x0, local copies, waits for them, and re-layouts: 12.4 us -> none  [the longest x2 5.86 us: per_device(): jnp.take(returned, destination, axis=0).reshape(tokens_here, 2, model_width)]
    unnamed x127 -> x78, local copies, waits for them, and re-layouts: 7.1 us -> 14.6 us
    mul x5 -> x0, local copies, waits for them, and re-layouts: 7.55 us -> none  [the longest x3 7.29 us: per_device(): route_weight[:, :, None] * out_grad[:, None, :].astype(jnp.float32)]
    reduce_scatter x3, waiting for transfers between devices: 39.3 us -> 45.9 us  [summed_rows(): total = lax.psum_scatter(total, axis, scatter_dimension=0, tiled=True)]
  transfers between devices with their start and end apart: 9 -> 5, of which waited for: 7 -> 4; matrix products, arithmetic and copies ran while one was open for 14% -> 11% of each run, Pallas kernels for 0% -> 32%
where the time goes in v1:
time: 322 us; the launch traced here: 320 us
  Pallas kernels  101 us (31%)
  waiting for transfers between devices  79.3 us (25%)
  blocking collectives  64.3 us (20%)
  other arithmetic  20.9 us (6%)
  local copies, waits for them, and re-layouts  19.3 us (6%)
  matrix products  19.1 us (6%)
  between operations  14.9 us (5%)
    pallas_call x1, Pallas kernels, expert_call(): pl.pallas_call(expert_kernel, out_shape=(jax.ShapeDtypeStruct((2048, 256)...  101 us
    reduce_scatter x3, waiting for transfers between devices, summed_rows(): total = lax.psum_scatter(total, axis, scatter_dimension=0, tiled=True)  45.9 us
    all_gather x4, blocking collectives, prefix_by_axis(): lax.all_gather(part.astype(kind), axis)  35.7 us
    all_gather x1, waiting for transfers between devices, prefix_by_axis_2(): lax.all_gather(part.astype(kind), axis)  33.3 us
    all_gather x3, blocking collectives, prefix_by_axis_2(): lax.all_gather(part.astype(kind), axis)  25.8 us
    unnamed x78, local copies, waits for them, and re-layouts  14.6 us
  transfers between devices with their start and end apart: 5, of which 4 were waited for; matrix products, arithmetic and copies ran while one was open for 11% of the time, Pallas kernels for 32%

profile of v1, /device:TPU:33, one launch (start us, length us, event | category | flops | bytes accessed | tf_op | source)
XLA Modules:
  0.0 319.6 jit_solution(14355395278154203315)
XLA Ops:
  7.3 0.9 copy.146
  8.8 1.3 dynamic-slice
  11.0 2.8 all-reduce
  14.5 1.0 copy.142
  15.5 1.0 copy.144
  16.5 8.0 %all-gather.3 = bf16[4,1,2]{2,1,0:T(2,128)(2,1)S(1)} all-gather(bf16[1,1,2]{2,1,0:T(2,128)(2,1)S(1)} %convert_bitcast_fusion.12), channel_id=1, replica_groups=mesh['sp_0'=8,'sp_1'=4,'sp_2'=2,'tp'=4] {'sp_1'}, dimensions={0}, use_global_device_ids=true | all-gather | bytes 20 | tf_op jit(solution)/shard_map/all_gather | solution.py:70
  25.7 0.8 fusion.97
  27.7 4.0 %all-gather = bf16[4,128,256]{2,1,0:T(8,128)(2,1)S(1)} all-gather(bf16[2,128,256]{2,1,0:T(8,128)(2,1)S(1)} %convolution_convert_fusion.1), channel_id=2, replica_groups=mesh['sp_0'=8,'sp_1'=4,'sp_2'=2,'tp'=4] {'sp_2'}, dimensions={0}, use_global_device_ids=true | all-gather | bytes 393216 | tf_op jit(solution)/shard_map/all_gather | solution.py:70
  32.3 0.8 fusion.46
  33.1 9.9 %all_gather.51 = bf16[4,2,128,256]{3,2,1,0:T(8,128)(2,1)S(1)} all-gather(bf16[1,2,128,256]{3,2,1,0:T(8,128)(2,1)S(1)} %fusion.46), channel_id=1, replica_groups=mesh['sp_0'=8,'sp_1'=4,'sp_2'=2,'tp'=4] {'sp_1'}, dimensions={0}, use_global_device_ids=true | all-gather | bytes 655360 | tf_op jit(solution)/shard_map/all_gather | solution.py:70
  43.0 0.8 fusion.20
  44.5 13.9 %all-gather.4 = bf16[8,1,2]{2,1,0:T(2,128)(2,1)} all-gather(bf16[1,1,2]{2,1,0:T(2,128)(2,1)S(1)} %get-tuple-element.87), channel_id=1, replica_groups=mesh['sp_0'=8,'sp_1'=4,'sp_2'=2,'tp'=4] {'sp_0'}, dimensions={0}, use_global_device_ids=true | all-gather | bytes 36 | tf_op jit(solution)/shard_map/all_gather | solution.py:70
  58.4 1.4 copy.140.routes
  59.8 1.4 copy.141.weight
  61.9 1.5 copy.149
  63.6 101.4 %shard_map.171 = (bf16[2048,256]{1,0:T(8,128)(2,1)}, bf16[2048,256]{1,0:T(8,128)(2,1)}, bf16[256,2048]{1,0:T(8,128)(2,1)}, bf16[2048,128]{1,0:T(8,128)(2,1)}) custom-call(bf16[128,2048]{1,0:T(8,128)(2,1)} %stream.1, bf16[128,2048]{1,0:T(8,128)(2,1)} %og.1, s32[128,2]{1,0:T(8,128)} %copy.140.routes, f32[128,2]{1,0:T(8,128)} %copy.141.weight, ...), custom_call_target="tpu_custom_call" | custom-call | tf_op jit(solution)/shard_map/pallas_call | solution.py:426
  166.8 1.1 convolution_multiply_fusion.1
  167.9 2.0 fusion.16
  170.2 1.0 multiply_reduce_fusion
  171.8 0.8 fusion.83
  172.7 3.7 %fusion.129 = f32[2048,512]{1,0:T(8,128)} fusion(bf16[2048,128]{1,0:T(8,128)(2,1)} %get-tuple-element.14, bf16[128,512]{0,1:T(8,128)(2,1)S(1)} %bitcast.441), kind=kOutput, calls=%fused_computation.268 | convolution fusion | flops 268435456 | bytes 4849664 | tf_op jit(solution)/shard_map/dot_general | solution.py:531
  177.5 1.6 fusion.130
  179.1 1.1 copy.154
  181.0 2.6 all-gather.2
  183.6 0.8 fusion.50
  184.5 10.9 %all_gather.57 = bf16[4,2,128,256]{3,2,1,0:T(8,128)(2,1)S(1)} all-gather(bf16[1,2,128,256]{3,2,1,0:T(8,128)(2,1)S(1)} %fusion.50), channel_id=1, replica_groups=mesh['sp_0'=8,'sp_1'=4,'sp_2'=2,'tp'=4] {'sp_1'}, dimensions={0}, use_global_device_ids=true | all-gather | bytes 655360 | tf_op jit(solution)/shard_map/all_gather | solution.py:97
  195.3 1.5 fusion.34
  196.9 12.3 %all-gather.5 = bf16[8,1,2]{2,1,0:T(2,128)(2,1)} all-gather(bf16[1,1,2]{2,1,0:T(2,128)(2,1)} %get-tuple-element.86), channel_id=1, replica_groups=mesh['sp_0'=8,'sp_1'=4,'sp_2'=2,'tp'=4] {'sp_0'}, dimensions={0}, use_global_device_ids=true | all-gather | bytes 36 | tf_op jit(solution)/shard_map/all_gather | solution.py:97
  209.2 1.5 copy.159
  210.7 1.2 fusion.102
  211.9 1.3 fusion.109
  213.2 1.8 convolution_multiply_fusion
  215.0 1.4 convolution_bitcast_fusion.5
  216.4 2.0 convolution_bitcast_fusion.1
  218.5 1.7 fusion.6
  220.2 6.8 %reduce-scatter.4.cloned.1.call-done = f32[256,512]{1,0:T(8,128)} async-done(((f32[2048,512]{1,0:T(8,128)}), f32[256,512]{1,0:T(8,128)}) %reduce-scatter.4.cloned.1.call-update) | async-done | bytes 524304 | tf_op jit(solution)/shard_map/reduce_scatter | solution.py:87
  227.1 1.9 convolution_bitcast_fusion.4
  229.0 33.3 %all-gather.11.cloned.1.call-done = bf16[8,2,128,256]{3,2,1,0:T(8,128)(2,1)} async-done(((bf16[1,2,128,256]{3,2,1,0:T(8,128)(2,1)}), bf16[8,2,128,256]{3,2,1,0:T(8,128)(2,1)}) %all-gather.11.cloned.1.call-update) | async-done | bytes 1048592 | tf_op jit(solution)/shard_map/all_gather | solution.py:97
  262.4 2.0 fusion.13
  264.4 1.2 fusion.4
  265.6 1.1 multiply_subtract_fusion
  266.9 0.8 copy.165
  267.6 22.8 %reduce-scatter.6.cloned.1.call-done = f32[64,512]{1,0:T(8,128)} async-done(((f32[256,512]{1,0:T(8,128)}), f32[64,512]{1,0:T(8,128)}) %reduce-scatter.6.cloned.1.call-update) | async-done | bytes 131088 | tf_op jit(solution)/shard_map/reduce_scatter | solution.py:87
  290.8 0.8 copy.166
  292.5 16.3 %reduce-scatter.8.cloned.1.call-done = f32[32,512]{1,0:T(8,128)} async-done(((f32[64,512]{1,0:T(8,128)}), f32[32,512]{1,0:T(8,128)}) %reduce-scatter.8.cloned.1.call-update) | async-done | bytes 65552 | tf_op jit(solution)/shard_map/reduce_scatter | solution.py:87
  308.8 2.4 copy.191
  311.1 1.0 copy.192
  312.1 1.0 copy.193
  (113 shorter events, 12.4 us)
Async XLA Ops:
  7.2 169.6 %copy-start = (bf16[2048,512]{1,0:T(8,128)(2,1)S(1)}, bf16[2048,512]{1,0:T(8,128)(2,1)}, u32[]{:S(2)}) copy-start(bf16[2048,512]{1,0:T(8,128)(2,1)} %param.20) | copy-start | bytes 6291460
  7.2 20.1 %copy-start.2 = (bf16[128,2,256]{2,1,0:T(2,128)(2,1)S(1)}, bf16[128,2,256]{2,1,0:T(2,128)(2,1)}, u32[]{:S(2)}) copy-start(bf16[128,2,256]{2,1,0:T(2,128)(2,1)} %param.18) | copy-start | bytes 393220
  7.2 160.7 %all-gather.9.cloned.1.call-start = ((), (), s32[]{:S(2)}) async-start(), calls=%async_computation.3 | async-start | bytes 1179648 | tf_op jit(solution)/shard_map/all_gather | solution.py:70
  8.4 18.7 %copy-start.14 = (f32[128,2]{0,1:T(2,128)}, f32[128,2]{0,1:T(2,128)S(1)}, u32[]{:S(2)}) copy-start(f32[128,2]{0,1:T(2,128)S(1)} %copy.147) | copy-start | bytes 3076
  8.6 18.5 %copy-start.30 = (f32[2]{0:T(128)}, f32[2]{0:T(128)S(1)}, u32[]{:S(2)}) copy-start(f32[2]{0:T(128)S(1)} %slice_reduce_fusion) | copy-start | bytes 28
  13.8 30.1 %copy-start.16 = (bf16[4]{0:T(256)(128)(2,1)}, bf16[4]{0:T(256)(128)(2,1)S(1)}, u32[]{:S(2)}) copy-start(bf16[4]{0:T(256)(128)(2,1)S(1)} %all-reduce) | copy-start | bytes 28
  24.5 35.3 %copy-start.12 = (bf16[4,1,2]{2,1,0:T(2,128)(2,1)}, bf16[4,1,2]{2,1,0:T(2,128)(2,1)S(1)}, u32[]{:S(2)}) copy-start(bf16[4,1,2]{2,1,0:T(2,128)(2,1)S(1)} %all-gather.3) | copy-start | bytes 52
  25.1 34.7 %copy-start.19 = (f32[2]{0:T(128)}, f32[2]{0:T(128)S(1)}, u32[]{:S(2)}) copy-start(f32[2]{0:T(128)S(1)} %get-tuple-element.90) | copy-start | bytes 28
  25.1 34.7 %copy-start.21 = (f32[2]{0:T(128)}, f32[2]{0:T(128)S(1)}, u32[]{:S(2)}) copy-start(f32[2]{0:T(128)S(1)} %get-tuple-element.91) | copy-start | bytes 28
  26.6 34.7 %copy-start.11 = (f32[128,64]{0,1:T(8,128)}, f32[128,64]{0,1:T(8,128)S(1)}, u32[]{:S(2)}) copy-start(f32[128,64]{0,1:T(8,128)S(1)} %get-tuple-element.94) | copy-start | bytes 98308
  26.8 16.2 %copy-start.29 = (f32[2]{0:T(128)S(1)}, f32[2]{0:T(128)}, u32[]{:S(2)}) copy-start(f32[2]{0:T(128)} %get-tuple-element.89) | copy-start | bytes 28
  27.1 137.9 %copy-start.4 = (f32[128,2,64,2]{0,3,2,1:T(2,128)}, f32[128,2,64,2]{0,3,2,1:T(2,128)S(1)}, u32[]{:S(2)}) copy-start(f32[128,2,64,2]{0,3,2,1:T(2,128)S(1)} %get-tuple-element.105) | copy-start | bytes 393220
  27.1 140.7 %copy-start.3 = (f32[128,2,64,2]{0,3,2,1:T(2,128)}, f32[128,2,64,2]{0,3,2,1:T(2,128)S(1)}, u32[]{:S(2)}) copy-start(f32[128,2,64,2]{0,3,2,1:T(2,128)S(1)} %get-tuple-element.104) | copy-start | bytes 393220
  27.2 34.1 %copy-start.31 = (f32[2]{0:T(128)S(1)}, f32[2]{0:T(128)}, u32[]{:S(2)}) copy-start(f32[2]{0:T(128)} %copy-done.30) | copy-start | bytes 28
  32.3 31.1 %copy-start.27 = (f32[2]{0:T(128)}, f32[2]{0:T(128)S(1)}, u32[]{:S(2)}) copy-start(f32[2]{0:T(128)S(1)} %get-tuple-element.85) | copy-start | bytes 28
  32.3 31.1 %copy-start.28 = (f32[2]{0:T(128)}, f32[2]{0:T(128)S(1)}, u32[]{:S(2)}) copy-start(f32[2]{0:T(128)S(1)} %get-tuple-element.99) | copy-start | bytes 28
  43.9 183.2 %reduce-scatter.4.cloned.1.call-start = ((), (), s32[]{:S(2)}) async-start(), calls=%async_computation.4 | async-start | bytes 4718592 | tf_op jit(solution)/shard_map/reduce_scatter | solution.py:87
  63.5 101.5 %copy-start.18 = (bf16[8,1,2]{2,1,0:T(2,128)(2,1)S(1)}, bf16[8,1,2]{2,1,0:T(2,128)(2,1)}, u32[]{:S(2)}) copy-start(bf16[8,1,2]{2,1,0:T(2,128)(2,1)} %all-gather.4) | copy-start | bytes 100
  63.5 102.0 %copy-start.13 = (bf16[4,1,2]{2,1,0:T(2,128)(2,1)S(1)}, bf16[4,1,2]{2,1,0:T(2,128)(2,1)}, u32[]{:S(2)}) copy-start(bf16[4,1,2]{2,1,0:T(2,128)(2,1)} %copy-done.12) | copy-start | bytes 52
  63.5 102.0 %copy-start.17 = (bf16[4]{0:T(256)(128)(2,1)S(1)}, bf16[4]{0:T(256)(128)(2,1)}, u32[]{:S(2)}) copy-start(bf16[4]{0:T(256)(128)(2,1)} %copy-done.16) | copy-start | bytes 28
  63.5 103.3 %copy-start.15 = (f32[128,2]{0,1:T(2,128)S(1)}, f32[128,2]{0,1:T(2,128)}, u32[]{:S(2)}) copy-start(f32[128,2]{0,1:T(2,128)} %copy-done.14) | copy-start | bytes 3076
  167.9 2.4 copy-start.5
  176.4 1.0 copy-start.1
  176.5 3.7 %copy-start.24 = (f32[2,128]{1,0:T(2,128)S(1)}, f32[2,128]{1,0:T(2,128)}, u32[]{:S(2)}) copy-start(f32[2,128]{1,0:T(2,128)} %get-tuple-element.95) | copy-start | bytes 3076
  176.5 4.1 %copy-start.25 = (f32[2,128]{1,0:T(2,128)S(1)}, f32[2,128]{1,0:T(2,128)}, u32[]{:S(2)}) copy-start(f32[2,128]{1,0:T(2,128)} %get-tuple-element.97) | copy-start | bytes 3076
  176.5 85.9 %all-gather.11.cloned.1.call-start = ((), (), s32[]{:S(2)}) async-start(), calls=%async_computation.7 | async-start | bytes 1179648 | tf_op jit(solution)/shard_map/all_gather | solution.py:97
  196.9 93.5 %reduce-scatter.6.cloned.1.call-start = ((), (), s32[]{:S(2)}) async-start(), calls=%async_computation.5 | async-start | bytes 655360 | tf_op jit(solution)/shard_map/reduce_scatter | solution.py:87
  215.0 47.3 %copy-start.20 = (f32[2]{0:T(128)S(1)}, f32[2]{0:T(128)}, u32[]{:S(2)}) copy-start(f32[2]{0:T(128)} %copy-done.19) | copy-start | bytes 28
  215.0 47.3 %copy-start.22 = (f32[2]{0:T(128)S(1)}, f32[2]{0:T(128)}, u32[]{:S(2)}) copy-start(f32[2]{0:T(128)} %copy-done.21) | copy-start | bytes 28
  215.0 47.3 %copy-start.26 = (f32[2]{0:T(128)S(1)}, f32[2]{0:T(128)}, u32[]{:S(2)}) copy-start(f32[2]{0:T(128)} %get-tuple-element.84) | copy-start | bytes 28
  216.4 48.0 %copy-start.23 = (f32[128,2]{0,1:T(2,128)S(1)}, f32[128,2]{0,1:T(2,128)}, u32[]{:S(2)}) copy-start(f32[128,2]{0,1:T(2,128)} %copy.159) | copy-start | bytes 3076
  227.1 81.7 %reduce-scatter.8.cloned.1.call-start = ((), (), s32[]{:S(2)}) async-start(), calls=%async_computation.6 | async-start | bytes 196608 | tf_op jit(solution)/shard_map/reduce_scatter | solution.py:87
  227.1 63.3 %copy-start.8 = (f32[128,2,256]{2,0,1:T(8,128)S(1)}, f32[128,2,256]{2,0,1:T(8,128)}, u32[]{:S(2)}) copy-start(f32[128,2,256]{2,0,1:T(8,128)} %convolution_bitcast_fusion.1) | copy-start | bytes 786436
  262.4 2.1 copy-start.9
  262.4 3.2 %copy-start.10 = (f32[128,2,128]{0,2,1:T(8,128)S(1)}, f32[128,2,128]{0,2,1:T(8,128)}, u32[]{:S(2)}) copy-start(f32[128,2,128]{0,2,1:T(8,128)} %fusion.6) | copy-start | bytes 393220
  292.5 19.6 %copy-start.6 = (bf16[256,2048]{1,0:T(8,128)(2,1)S(1)}, bf16[256,2048]{1,0:T(8,128)(2,1)}, u32[]{:S(2)}) copy-start(bf16[256,2048]{1,0:T(8,128)(2,1)} %get-tuple-element.13) | copy-start | bytes 3145732
  308.8 2.4 copy-start.7
Sparse Core Ops, SparseCore 0:
  44.0 38.1 all-gather.8
  176.6 50.3 reduce-scatter.3
  228.8 33.4 all-gather.10
  264.7 25.6 reduce-scatter.5
  293.3 15.4 reduce-scatter.7

commit v2 on v0

v2 whole, which is shorter than its diff:
```python
import types

import jax
import jax.numpy as jnp
import numpy as np
from jax import lax
from jax.experimental import pallas as pl
from jax.experimental.pallas import tpu as pltpu
from jax.sharding import PartitionSpec as P

CLAMP_LIMIT = 7.0
GATE_SLOPE = 1.702
EPSILON = 1e-06
MESH = pl.DeviceIdType.MESH
BF = jnp.bfloat16
F32 = jnp.float32
HIGHEST = lax.Precision.HIGHEST

N_SP, N_TP = 64, 4
TOK, D, KD, VD = 128, 2048, 128, 256
QUART = D // N_TP
SHIFTS = (1, 7, 2, 6, 3, 5, 4)
WHOLE = (1, 7, 0)
BOTH = (1, 7)
PARTS = (1, 7, 2, 6, 3, 5, 4)
QUEUE = (
    (1, False),
    (7, False),
    (2, False),
    (6, False),
    (1, True),
    (7, True),
    (3, False),
    (5, False),
    (0, True),
    (4, False),
)
FIRST = 0
CHUNKS = (
    ((1, 0, 8), (7, 0, 8)),
    ((2, 0, 8), (6, 0, 8)),
    ((0, 0, 4), (0, 4, 4)),
    ((3, 0, 8), (5, 0, 8)),
    ((4, 0, 4), (4, 4, 4)),
)


def dot(a, b, ca, cb, precision=None):
    return lax.dot_general(
        a, b, (((ca,), (cb,)), ((), ())), preferred_element_type=F32, precision=precision
    )


def dotb(a, b, ca, cb):
    return dot(a.astype(BF), b.astype(BF), ca, cb)


def remote(src, dst, send_sem, recv_sem, device):
    pltpu.make_async_remote_copy(
        src_ref=src,
        dst_ref=dst,
        send_sem=send_sem,
        recv_sem=recv_sem,
        device_id=device,
        device_id_type=MESH,
    ).start()


def take(ref, sem):
    pltpu.make_async_copy(ref, ref, sem).wait()


def iota(shape, dim):
    return lax.broadcasted_iota(jnp.int32, shape, dim)


INPUTS = (
    "stream",
    "og",
    "in_routes",
    "in_weight",
    "in_queries",
    "in_keys",
    "in_values",
    "in_decay",
    "out_proj",
    "gate_w",
    "up_w",
    "down_w",
    "in_starts",
    "in_places",
)
SMALL = {
    "routes": ((2, TOK), jnp.int32),
    "weight": ((2, TOK), F32),
    "decay": ((2, TOK), F32),
    "starts": ((2 * N_SP, KD), F32),
    "places": ((2 * TOK, KD), F32),
    "queries": ((TOK, 2, KD), BF),
    "keys": ((TOK, 2, KD), BF),
    "values": ((TOK, 2, VD), BF),
}
OUTPUTS = {
    "o_gate": ((1, D, 256), BF),
    "o_up": ((1, D, 256), BF),
    "o_down": ((1, 256, D), BF),
    "o_proj": ((32, 512), F32),
    "o_query": ((TOK, 2, KD), BF),
    "o_key": ((TOK, 2, KD), BF),
    "o_value": ((TOK, 2, VD), BF),
}
BUFFERS = {
    **SMALL,
    "sf": ((TOK, D), BF),
    "of": ((TOK, D), BF),
    "ws": ((512, 1), F32),
    "w": ((D, 512), BF),
    "d": ((256, D), BF),
    "op": ((D, 512), BF),
    "pm": ((512, TOK), BF),
    "send": ((N_SP, 16, QUART), BF),
    "whole": ((3, 8, 4, 16, QUART), BF),
    "rg": ((N_SP, 4, 16, QUART), BF),
    "gu": ((512, 512), BF),
    "ac": ((512, 256), BF),
    "bk": ((4, N_SP, 8, QUART), BF),
    "xin": ((6, 5, 8, 8, QUART), BF),
    "acc": ((2, 5, 8, 8, QUART), BF),
    "fin": ((N_SP, 8, QUART), BF),
    "ret": ((N_SP, 8, QUART), BF),
    "rt": ((N_SP, 32, TOK), BF),
    "qr": ((2, TOK, KD), F32),
    "kr": ((2, TOK, KD), F32),
    "vh": ((2, TOK, VD), BF),
    "mask": ((2, TOK, TOK), F32),
    "wt": ((2, TOK, TOK), BF),
    "nrm": ((2, TOK, VD), F32),
    "inv": ((2, TOK, 1), F32),
    "phd": ((2, TOK, 1), F32),
    "rem": ((2, TOK, 1), F32),
    "sa": ((2, 8, 32, VD), BF),
    "ra": ((2, 8, 32, VD), BF),
    "pp": ((2, 8, 32, VD), F32),
    "sb": ((2, 32, VD), BF),
    "rb": ((2, 8, 32, VD), BF),
    "sc": ((2, 8, 32, VD), BF),
    "rc": ((2, 8, 32, VD), BF),
    "tmine": ((2, VD), F32),
    "tplane": ((2, VD), F32),
    "ta": ((8, 2, VD), F32),
    "tb": ((8, 2, VD), F32),
    "nb": ((TOK, 512), BF),
    "na": ((8, TOK, 512), BF),
    "rr": ((8, 8, 32, TOK), BF),
    "zp": ((8, 32, 512), BF),
    "rz": ((8, 32, 512), BF),
}
SEMAPHORES = {
    "load": (14,),
    "d_send": (),
    "d_recv": (2, 8),
    "x_send": (),
    "x_recv": (4, 8),
    "r_send": (),
    "r_recv": (6, 5),
    "t_send": (),
    "t_recv": (),
    "g_send": (),
    "g_recv": (6,),
    "s_send": (2, 3),
    "s_recv": (2, 3),
    "u_send": (2,),
    "u_recv": (2,),
    "n_send": (),
    "n_recv": (3,),
    "p_send": (2,),
    "p_recv": (),
    "q_recv": (4,),
}
NAMES = (*INPUTS, *OUTPUTS, *BUFFERS, *SEMAPHORES)


def kernel(*refs):
    r = types.SimpleNamespace(**dict(zip(NAMES, refs, strict=True)))
    me = lax.axis_index("sp")
    x = lax.axis_index("tp")
    z, j = me // 8, me % 8
    other = j + 1 - 2 * (j % 2)
    right, left, far = (x + 1) % 4, (x + 3) % 4, (x + 2) % 4

    def plane(dz):
        return (z + dz) % 8

    cols = pl.ds(pl.multiple_of(x * QUART, QUART), QUART)
    barrier = pltpu.get_barrier_semaphore()

    def hello(k, _):
        pl.semaphore_signal(barrier, inc=1, device_id=((me + k) % 64, x), device_id_type=MESH)
        return 0

    lax.fori_loop(32, 64, hello, 0)
    lax.fori_loop(1, 32, hello, 0)
    for peer in (right, left, far):
        pl.semaphore_signal(barrier, inc=1, device_id=(me, peer), device_id_type=MESH)

    copies = [
        (r.in_routes, r.routes),
        (r.in_weight, r.weight),
        (r.stream, r.sf),
        (r.og, r.of),
        *((getattr(r, "in_" + name), getattr(r, name)) for name in list(SMALL)[2:]),
        (r.gate_w.at[0], r.w.at[:, pl.ds(0, 256)]),
        (r.up_w.at[0], r.w.at[:, pl.ds(256, 256)]),
        (r.down_w.at[0], r.d),
        (r.out_proj, r.op),
    ]
    loads = [pltpu.make_async_copy(*c, r.load.at[i]) for i, c in enumerate(copies)]
    for c in loads:
        c.start()

    rows, lanes = iota((TOK, TOK), 0), iota((TOK, TOK), 1)
    loads[0].wait()
    loads[1].wait()
    ids = r.routes[...].astype(F32)
    wrow = r.weight[...]
    expert = iota((64, TOK), 0).astype(F32)
    named0 = (expert == ids[0:1]).astype(F32)
    named1 = (expert == ids[1:2]).astype(F32)
    before = dotb(named0 + named1, (rows < lanes).astype(F32), 1, 0)
    dest0 = ids[0:1] * 8.0 + jnp.sum(named0 * before, axis=0, keepdims=True)
    dest1 = ids[1:2] * 8.0 + jnp.sum(named1 * before, axis=0, keepdims=True)
    slot = iota((512, TOK), 0).astype(F32)
    at0 = (slot == dest0).astype(F32)
    at1 = (slot == dest1).astype(F32)
    wslot = jnp.sum(at0 * wrow[0:1] + at1 * wrow[1:2], axis=1, keepdims=True)
    place = (at0 + at1).astype(BF)
    r.pm[...] = place
    r.ws[...] = wslot
    loads[2].wait()
    r.send[:, 0:8, :] = dot(place, r.sf[:, cols], 1, 0).reshape(64, 8, QUART).astype(BF)
    loads[3].wait()
    r.send[:, 8:16, :] = (dot(place, r.of[:, cols], 1, 0) * wslot).reshape(64, 8, QUART).astype(BF)

    pl.semaphore_wait(barrier, 66)

    mine, others = j // 4 * 4, 4 - j // 4 * 4

    def dispatch(dz, whole):
        def send_to(m):
            p = plane(dz) * 8 + m
            if whole:
                block, slot_of = r.whole.at[WHOLE.index(dz), m], r.rg.at[me]
            else:
                block, slot_of = r.send.at[p], r.rg.at[me, x]
            remote(block, slot_of, r.d_send, r.d_recv.at[int(whole), dz], (p, x))

        def one(k, _):
            send_to((j + k) % 8)
            return 0

        def one_of_half(k, _):
            send_to((mine if whole else others) + (j + k) % 4)
            return 0

        if dz in BOTH:
            lax.fori_loop(0, 4, one_of_half, 0)
        else:
            lax.fori_loop(1 if dz == 0 else 0, 8, one, 0)

    def build_whole():
        for i, dz in enumerate(WHOLE):
            at = pl.ds(pl.multiple_of(plane(dz) * 64, 64), 64)
            slots, scale = r.pm[at, :], r.ws[at, :]
            for q in range(4):
                these = slice(q * QUART, (q + 1) * QUART)
                rows_q = dot(slots, r.sf[:, these], 1, 0)
                grads_q = dot(slots, r.of[:, these], 1, 0) * scale
                r.whole[i, :, q, 0:8, :] = rows_q.reshape(8, 8, QUART).astype(BF)
                r.whole[i, :, q, 8:16, :] = grads_q.reshape(8, 8, QUART).astype(BF)

    first_whole = [whole for _, whole in QUEUE].index(True)
    for at, (dz, whole) in enumerate(QUEUE):
        if at == first_whole:
            build_whole()
        dispatch(dz, whole)
    r.rg[me] = r.whole[WHOLE.index(0), j]

    odd = lanes % 2 == 1

    def angles():
        ca, sa = r.starts[pl.ds(me, 1), :], r.starts[pl.ds(me + 64, 1), :]
        cb, sb = r.places[0:128, :], r.places[128:256, :]
        return ca * cb - sa * sb, jnp.where(odd, 1.0, -1.0) * (sa * cb + ca * sb)

    def turn(field, cosines, sines):
        partner = jnp.where(odd, pltpu.roll(field, 1, 1), pltpu.roll(field, TOK - 1, 1))
        return field * cosines + partner * sines

    def apart():
        a, b = iota((256, 256), 0), iota((256, 256), 1)
        return (b == 2 * (a % 128) + a // 128).astype(BF)

    for c in loads[4:10]:
        c.wait()
    cosines, sines = angles()
    split = apart()
    q2 = dot(split, r.queries[...].reshape(256, KD), 1, 0)
    k2 = dot(split, r.keys[...].reshape(256, KD), 1, 0)
    v2 = [dot(split, r.values[:, :, 128 * i : 128 * i + 128].reshape(256, 128), 1, 0) for i in (0, 1)]
    decay = r.decay[...]
    cum_row = dot(decay, (rows <= lanes).astype(F32), 1, 0, HIGHEST)
    cum_col = dot((rows >= lanes).astype(F32), decay, 1, 1, HIGHEST)
    causal = rows >= lanes
    for h in range(2):
        at = slice(128 * h, 128 * h + 128)
        q = turn(q2[at], cosines, sines)
        k = turn(k2[at], cosines, sines) * KD ** (-0.5)
        r.qr[h] = q
        r.kr[h] = k
        r.vh[h, :, 0:128] = v2[0][at].astype(BF)
        r.vh[h, :, 128:256] = v2[1][at].astype(BF)
        col = cum_col[:, h : h + 1]
        total = cum_col[127:128, h : h + 1]
        rem = jnp.exp(total - col)
        r.phd[h] = jnp.exp(col)
        r.rem[h] = rem
        diff = col - cum_row[h : h + 1, :]
        mask = jnp.where(causal, jnp.exp(jnp.where(causal, diff, 0.0)), 0.0)
        r.mask[h] = mask
        state = dotb(k * rem, r.vh[h], 0, 0)
        r.sa[0, pl.ds(4 * h, 4)] = state.astype(BF).reshape(4, 32, VD)
        r.tmine[h : h + 1, :] = jnp.broadcast_to(total, (1, VD))

    def within(src, dst, send_sem, recv_sem):
        def one(k, _):
            m = (j + k) % 8
            remote(src(m), dst(j), send_sem, recv_sem, (z * 8 + m, x))
            return 0

        lax.fori_loop(1, 8, one, 0)

    def over_z(src, dst, send_sem, recv_sem):
        for dz in PARTS:
            remote(src(plane(dz)), dst(z), send_sem, recv_sem, (plane(dz) * 8 + j, x))

    def stage_a(way):
        within(
            lambda m: r.sa.at[way, m],
            lambda m: r.ra.at[way, m],
            r.s_send.at[way, 0],
            r.s_recv.at[way, 0],
        )
        r.ra[way, j] = r.sa[way, j]
        if way == 0:
            within(lambda m: r.tmine, lambda m: r.ta.at[m], r.u_send.at[0], r.u_recv.at[0])
            r.ta[j] = r.tmine[...]

    head = pl.ds(j // 4, 1)

    def stage_b(way):
        take(r.ra.at[way, pl.ds(0, 7)], r.s_recv.at[way, 0])
        if way == 0:
            take(r.ta.at[pl.ds(0, 7)], r.u_recv.at[0])
            total = r.ta[0]
            for m in range(1, 8):
                total = total + r.ta[m]
            r.tplane[...] = total
        run = jnp.zeros((32, VD), F32)
        for m in range(8) if way == 0 else reversed(range(8)):
            r.pp[way, m] = run
            run = jnp.exp(r.ta[m, head, :]) * run + r.ra[way, m].astype(F32)
        r.sb[way] = run.astype(BF)
        over_z(
            lambda p: r.sb.at[way],
            lambda p: r.rb.at[way, p],
            r.s_send.at[way, 1],
            r.s_recv.at[way, 1],
        )
        r.rb[way, z] = r.sb[way]
        if way == 0:
            over_z(lambda p: r.tplane, lambda p: r.tb.at[p], r.u_send.at[1], r.u_recv.at[1])
            r.tb[z] = r.tplane[...]

    def stage_c(way):
        take(r.rb.at[way, pl.ds(0, 7)], r.s_recv.at[way, 1])
        if way == 0:
            take(r.tb.at[pl.ds(0, 7)], r.u_recv.at[1])
        run = jnp.zeros((32, VD), F32)
        for p in range(8) if way == 0 else reversed(range(8)):
            passed = (p < z) if way == 0 else (p > z)
            new = jnp.exp(r.tb[p, head, :]) * run + r.rb[way, p].astype(F32)
            run = jnp.where(passed, new, run)
        logs = jnp.zeros((1, VD), F32)
        for m in range(8) if way == 0 else reversed(range(8)):
            r.sc[way, m] = (jnp.exp(logs) * run + r.pp[way, m]).astype(BF)
            logs = logs + r.ta[m, head, :]
        within(
            lambda m: r.sc.at[way, m],
            lambda m: r.rc.at[way, m],
            r.s_send.at[way, 2],
            r.s_recv.at[way, 2],
        )
        r.rc[way, j] = r.sc[way, j]

    def state_of(way, h):
        return r.rc[way, pl.ds(4 * h, 4)].reshape(128, VD)

    def normalise():
        take(r.rc.at[0, pl.ds(0, 7)], r.s_recv.at[0, 2])
        for h in range(2):
            q, k, v = r.qr[h], r.kr[h], r.vh[h]
            weights = (dotb(q, k, 1, 1) * r.mask[h]).astype(BF)
            r.wt[h] = weights
            kept = dot(weights, v, 1, 0) + r.phd[h] * dotb(q, state_of(0, h), 1, 0)
            inv = lax.rsqrt(jnp.mean(kept * kept, axis=1, keepdims=True) + EPSILON)
            r.inv[h] = inv
            r.nrm[h] = kept * inv
            r.nb[:, 256 * h : 256 * h + 256] = (kept * inv).astype(BF)
        r.na[j] = r.nb[...]
        remote(r.nb, r.na.at[j], r.n_send, r.n_recv.at[0], (z * 8 + other, x))
        for k in range(1, 4):
            m = (j + 2 * k) % 8
            remote(r.nb, r.na.at[j], r.n_send, r.n_recv.at[1], (z * 8 + m, x))

    def relay():
        take(r.na.at[pl.ds(0, 3)], r.n_recv.at[1])
        for k in range(1, 4):
            m = (j + 2 * k) % 8
            remote(r.na.at[m], r.na.at[m], r.n_send, r.n_recv.at[2], (z * 8 + other, x))

    def senders(dz):
        if dz in BOTH:
            return plane(8 - dz) * 8 + others, 4
        return plane(8 - dz) * 8, 8

    def group(q, dz):
        first, n = senders(dz)
        return r.rg.at[pl.ds(first, n), q]

    def half(q, dz, h):
        first, n = senders(dz)
        return r.rg.at[pl.ds(first + h * (n // 2), n // 2), q]

    def spread(dz):
        take(group(x, dz), r.d_recv.at[0, dz])
        remote(group(x, dz), group(x, dz), r.x_send, r.x_recv.at[0, dz], (me, right))
        remote(group(x, dz), group(x, dz), r.x_send, r.x_recv.at[1, dz], (me, left))

    def pass_on(dz):
        take(group(left, dz), r.x_recv.at[0, dz])
        remote(half(left, dz, 0), half(left, dz, 0), r.x_send, r.x_recv.at[2, dz], (me, right))
        take(group(right, dz), r.x_recv.at[1, dz])
        remote(half(right, dz, 1), half(right, dz, 1), r.x_send, r.x_recv.at[3, dz], (me, left))

    def complete(dz):
        if dz in PARTS:
            take(half(far, dz, 0), r.x_recv.at[2, dz])
            take(half(far, dz, 1), r.x_recv.at[3, dz])
        if dz in BOTH:
            take(r.rg.at[pl.ds(plane(8 - dz) * 8 + mine, 4)], r.d_recv.at[1, dz])
        elif dz in WHOLE:
            take(r.rg.at[pl.ds(0, 7)], r.d_recv.at[1, dz])

    def block(m, part):
        dz, first, n = CHUNKS[m][part]
        return plane(8 - dz) * 8 + first, n

    def experts(m):
        for dz in dict.fromkeys(c[0] for c in CHUNKS[m]):
            complete(dz)
        if m == FIRST:
            for c in loads[10:]:
                c.wait()
        (fa, na), (fb, nb) = block(m, 0), block(m, 1)

        def both(q, part):
            these = pl.ds(8 * part, 8)
            a = r.rg[pl.ds(fa, na), q, these, :].reshape(8 * na, QUART)
            b = r.rg[pl.ds(fb, nb), q, these, :].reshape(8 * nb, QUART)
            return jnp.concatenate([a, b], axis=0)

        pre = dot(both(0, 0), r.w[0:QUART, :], 1, 0)
        back = dot(both(0, 1), r.d[:, 0:QUART], 1, 1)
        for q in range(1, 4):
            pre = pre + dot(both(q, 0), r.w[q * QUART : (q + 1) * QUART, :], 1, 0)
            back = back + dot(both(q, 1), r.d[:, q * QUART : (q + 1) * QUART], 1, 1)
        gate_pre, up_pre = pre[:, 0:256], pre[:, 256:512]
        gate_clip = jnp.minimum(gate_pre, CLAMP_LIMIT)
        up_clip = jnp.clip(up_pre, -CLAMP_LIMIT, CLAMP_LIMIT)
        sig = jax.nn.sigmoid(GATE_SLOPE * gate_clip)
        activated = (gate_clip * sig * (up_clip + 1.0)).astype(BF)
        slope = sig + GATE_SLOPE * gate_clip * sig * (1.0 - sig)
        gate_g = jnp.where(gate_pre < CLAMP_LIMIT, back * (up_clip + 1.0) * slope, 0.0).astype(BF)
        up_g = jnp.where(jnp.abs(up_pre) < CLAMP_LIMIT, back * gate_clip * sig, 0.0).astype(BF)
        both_g = jnp.concatenate([gate_g, up_g], axis=1)
        for lo, first, n in ((0, fa, na), (8 * na, fb, nb)):
            at = pl.ds(pl.multiple_of(first * 8, 32), 8 * n)
            r.gu[at, :] = both_g[lo : lo + 8 * n]
            r.ac[at, :] = activated[lo : lo + 8 * n]
        for q in range(4):
            out = dot(both_g, r.w[q * QUART : (q + 1) * QUART, :], 1, 1).astype(BF)
            for lo, first, n in ((0, fa, na), (8 * na, fb, nb)):
                r.bk[q, pl.ds(first, n)] = out[lo : lo + 8 * n].reshape(n, 8, QUART)

        pa, pb = pl.ds(fa, na), pl.ds(fb, nb)
        for k, rows_of, to in (
            (0, r.bk.at[far, pa], right),
            (1, r.bk.at[far, pb], left),
            (2, r.bk.at[left, pa], left),
            (3, r.bk.at[right, pb], right),
        ):
            space = r.xin.at[k, m, pl.ds(0, nb if k % 2 else na)]
            remote(rows_of, space, r.r_send, r.r_recv.at[k, m], (me, to))

    def forward(m):
        for part, mine_of, to in ((0, right, right), (1, left, left)):
            first, n = block(m, part)
            at, here = pl.ds(0, n), pl.ds(first, n)
            take(r.xin.at[part, m, at], r.r_recv.at[part, m])
            r.acc[part, m, at] = (
                r.xin[part, m, at].astype(F32) + r.bk[mine_of, here].astype(F32)
            ).astype(BF)
            remote(
                r.acc.at[part, m, at],
                r.xin.at[4 + part, m, at],
                r.r_send,
                r.r_recv.at[4 + part, m],
                (me, to),
            )

    def finish(m):
        for part in range(2):
            dz = CHUNKS[m][part][0]
            first, n = block(m, part)
            at, here = pl.ds(0, n), pl.ds(first, n)
            direct, summed = 2 + part, 4 + part
            take(r.xin.at[direct, m, at], r.r_recv.at[direct, m])
            take(r.xin.at[summed, m, at], r.r_recv.at[summed, m])
            r.fin[here] = (
                r.bk[x, here].astype(F32)
                + r.xin[direct, m, at].astype(F32)
                + r.xin[summed, m, at].astype(F32)
            ).astype(BF)

            def one(k, _, first=first, n=n, dz=dz):
                p = first + (j + k) % n
                if dz == 0:

                    @pl.when(p != me)
                    def _():
                        remote(r.fin.at[p], r.ret.at[me], r.t_send, r.t_recv, (p, x))

                else:
                    remote(r.fin.at[p], r.ret.at[me], r.t_send, r.t_recv, (p, x))
                return 0

            lax.fori_loop(0, n, one, 0)
            if dz == 0:

                @pl.when((me >= first) & (me < first + n))
                def _():
                    r.ret[me] = r.fin[me]

    def weight_grads(q):
        at = pl.ds(q * QUART, QUART)
        rows_q = r.rg[:, q, 0:8, :].reshape(512, QUART)
        grads_q = r.rg[:, q, 8:16, :].reshape(512, QUART)
        both = dot(rows_q, r.gu[...], 0, 0).astype(BF)
        r.o_gate[0, at, :] = both[:, 0:256]
        r.o_up[0, at, :] = both[:, 256:512]
        r.o_down[0, :, at] = dot(r.ac[...], grads_q, 0, 0).astype(BF)

    spread(1)
    spread(7)
    stage_a(0)
    pass_on(1)
    pass_on(7)
    spread(2)
    spread(6)
    pass_on(2)
    pass_on(6)
    experts(0)
    spread(3)
    forward(0)
    spread(5)
    pass_on(3)
    experts(1)
    pass_on(5)
    finish(0)
    spread(4)
    forward(1)
    stage_b(0)
    experts(2)
    experts(3)
    pass_on(4)
    finish(1)
    stage_c(0)
    forward(2)
    forward(3)
    experts(4)
    finish(2)
    normalise()
    finish(3)
    weight_grads(0)
    forward(4)
    weight_grads(1)
    finish(4)
    relay()
    weight_grads(2)
    weight_grads(3)

    def quarter(q):
        return pl.ds(q * 16, 16)

    take(r.ret.at[pl.ds(0, 63)], r.t_recv)
    same = (rows == lanes).astype(BF)
    resid = dot(r.ret[...].reshape(512, QUART), r.pm[...], 0, 0) + dot(r.of[:, cols], same, 0, 0)
    r.rt[quarter(x)] = resid.astype(BF).reshape(16, 32, TOK)
    def part_of(q, h):
        return r.rt.at[pl.ds(q * 16 + 8 * h, 8)]

    for k, (h, peer) in enumerate(((0, right), (1, left), (1, right), (0, left))):
        remote(part_of(x, h), part_of(x, h), r.g_send, r.g_recv.at[k], (me, peer))

    def give(i, q):
        def one(k, _):
            m = (j + k) % 8
            for p in (2 * q, 2 * q + 1):
                remote(
                    r.rt.at[p * 8 + m],
                    r.rr.at[j, p],
                    r.p_send.at[0],
                    r.q_recv.at[i],
                    (z * 8 + m, x),
                )
            return 0

        lax.fori_loop(1, 8, one, 0)
        for p in (2 * q, 2 * q + 1):
            r.rr[j, p] = r.rt[p * 8 + j]

    give(0, x)

    def share(q):
        rows_q = pl.ds(pl.multiple_of(q * QUART, QUART), QUART)
        return dot(r.rt[quarter(q)].reshape(QUART, TOK), r.op[rows_q, :], 0, 0)

    take(part_of(left, 0), r.g_recv.at[0])
    remote(part_of(left, 0), part_of(left, 0), r.g_send, r.g_recv.at[4], (me, right))
    take(part_of(right, 1), r.g_recv.at[1])
    remote(part_of(right, 1), part_of(right, 1), r.g_send, r.g_recv.at[5], (me, left))
    take(part_of(left, 1), r.g_recv.at[2])
    take(part_of(right, 0), r.g_recv.at[3])
    give(1, left)
    give(2, right)
    normed_grad = share(x) + share(left) + share(right)
    take(part_of(far, 0), r.g_recv.at[4])
    take(part_of(far, 1), r.g_recv.at[5])
    normed_grad = normed_grad + share(far)

    grads = []
    for h in range(2):
        normed = r.nrm[h]
        ng = normed_grad[:, 256 * h : 256 * h + 256]
        g = r.inv[h] * (ng - normed * jnp.mean(ng * normed, axis=1, keepdims=True))
        grads.append(g.astype(BF))
        inner = dotb(r.qr[h] * r.phd[h], grads[h], 0, 0)
        r.sa[1, pl.ds(4 * h, 4)] = inner.astype(BF).reshape(4, 32, VD)
    stage_a(1)
    give(3, far)

    query_parts, key_parts, value_parts = [], [], []
    for h in range(2):
        q, k, v, g = r.qr[h], r.kr[h], r.vh[h], grads[h]
        score = (dot(g, v, 1, 1) * r.mask[h]).astype(BF)
        query_parts.append(dotb(score, k, 1, 0) + r.phd[h] * dot(g, state_of(0, h), 1, 1))
        key_parts.append(dotb(score, q, 0, 0))
        value_parts.append(dot(r.wt[h], g, 0, 0))

    def together(parts):
        return dot(split, jnp.concatenate(parts, axis=0).astype(BF), 0, 0).astype(BF)

    r.o_query[...] = together([turn(p, cosines, -sines) for p in query_parts]).reshape(TOK, 2, KD)

    def project(*pieces):
        for i, _ in pieces:
            take(r.rt.at[pl.ds(0, 14)], r.q_recv.at[i])

        def rows_of(m):
            return jnp.concatenate(
                [r.rr[m, pl.ds(2 * q, 2)].reshape(64, TOK) for _, q in pieces], axis=0
            )

        part = dot(rows_of(0), r.na[0], 1, 0)
        for m in range(1, 8):
            part = part + dot(rows_of(m), r.na[m], 1, 0)
        for k, (_, q) in enumerate(pieces):
            r.zp[pl.ds(2 * q, 2)] = part[64 * k : 64 * k + 64].astype(BF).reshape(2, 32, 512)
            for to in (2 * q, 2 * q + 1):

                @pl.when(to != z)
                def _(to=to):
                    remote(r.zp.at[to], r.rz.at[z], r.p_send.at[1], r.p_recv, (to * 8 + j, x))

                @pl.when(to == z)
                def _():
                    r.rz[z] = r.zp[z]

    stage_b(1)
    take(r.nb, r.n_recv.at[0])
    take(r.na.at[pl.ds(0, 3)], r.n_recv.at[2])
    project((0, x), (1, left), (2, right), (3, far))
    stage_c(1)

    take(r.rz.at[pl.ds(0, 7)], r.p_recv)
    total = r.rz[0].astype(F32)
    for p in range(1, 8):
        total = total + r.rz[p].astype(F32)
    r.o_proj[...] = total

    take(r.rc.at[1, pl.ds(0, 7)], r.s_recv.at[1, 2])
    for h in range(2):
        future = state_of(1, h)
        key_parts[h] = key_parts[h] + r.rem[h] * dot(r.vh[h], future, 1, 1)
        value_parts[h] = value_parts[h] + r.rem[h] * dotb(r.kr[h], future, 1, 0)
    r.o_key[...] = together(
        [turn(p, cosines, -sines) * KD ** (-0.5) for p in key_parts]
    ).reshape(TOK, 2, KD)
    for i in range(2):
        at = slice(128 * i, 128 * i + 128)
        r.o_value[:, :, at] = together([p[:, at] for p in value_parts]).reshape(TOK, 2, 128)

    take(r.rg.at[pl.ds(0, 27)], r.d_send)
    take(r.rg.at[pl.ds(0, 36)], r.x_send)
    take(r.xin.at[:, pl.ds(0, 4)], r.r_send)
    take(r.fin.at[pl.ds(0, 63)], r.t_send)
    take(r.rt.at[pl.ds(0, 48)], r.g_send)
    for way in range(2):
        take(r.sa.at[way, pl.ds(0, 7)], r.s_send.at[way, 0])
        take(r.rb.at[way, pl.ds(0, 7)], r.s_send.at[way, 1])
        take(r.sc.at[way, pl.ds(0, 7)], r.s_send.at[way, 2])
    take(r.ta.at[pl.ds(0, 7)], r.u_send.at[0])
    take(r.tb.at[pl.ds(0, 7)], r.u_send.at[1])
    take(r.na.at[pl.ds(0, 7)], r.n_send)
    take(r.rr.at[pl.ds(0, 7)], r.p_send.at[0])
    take(r.zp.at[pl.ds(0, 7)], r.p_send.at[1])


def write_out(*refs):
    n = len(OUTPUTS)
    copies = [pltpu.make_async_copy(refs[i], refs[n + i], refs[2 * n].at[i]) for i in range(n)]
    for c in copies:
        c.start()
    for c in copies:
        c.wait()


def rotation_tables():
    frequency = np.repeat(10000.0 ** (-np.linspace(0.0, 1.0, KD // 2)), 2)[None, :]
    starts = np.arange(N_SP)[:, None] * TOK * frequency
    places = np.arange(TOK)[:, None] * frequency
    return tuple(
        np.concatenate([np.cos(a), np.sin(a)]).astype(np.float32) for a in (starts, places)
    )


def per_device(
    stream,
    out_grad,
    routes,
    route_weight,
    queries,
    key_vectors,
    value_vectors,
    log_decay,
    out_proj,
    gate_weight,
    up_weight,
    down_weight,
):
    starts, places = rotation_tables()
    anywhere = pl.BlockSpec(memory_space=pltpu.HBM)
    local = pl.BlockSpec(memory_space=pltpu.VMEM)
    results = pl.pallas_call(
        kernel,
        out_shape=tuple(pltpu.VMEM(*o) for o in OUTPUTS.values()),
        in_specs=(anywhere,) * len(INPUTS),
        out_specs=(local,) * len(OUTPUTS),
        scratch_shapes=[
            *(pltpu.VMEM(*b) for b in BUFFERS.values()),
            *(pltpu.SemaphoreType.DMA(s) if s else pltpu.SemaphoreType.DMA for s in SEMAPHORES.values()),
        ],
        compiler_params=pltpu.CompilerParams(
            collective_id=0, has_side_effects=True, vmem_limit_bytes=60 * 1024 * 1024
        ),
    )(
        stream,
        out_grad,
        routes.T,
        route_weight.T,
        queries,
        key_vectors,
        value_vectors,
        log_decay.T,
        out_proj,
        gate_weight,
        up_weight,
        down_weight,
        jnp.asarray(starts),
        jnp.asarray(places),
    )
    return pl.pallas_call(
        write_out,
        out_shape=tuple(jax.ShapeDtypeStruct(*o) for o in OUTPUTS.values()),
        in_specs=(local,) * len(OUTPUTS),
        out_specs=(anywhere,) * len(OUTPUTS),
        scratch_shapes=[pltpu.SemaphoreType.DMA((len(OUTPUTS),))],
        compiler_params=pltpu.CompilerParams(vmem_limit_bytes=1024 * 1024),
    )(*(pltpu.with_memory_space_constraint(a, pltpu.VMEM) for a in results))


def solution(mesh):
    by_position, by_head = P("sp", None), P("sp", "tp", None)
    columns, rows = P("sp", None, "tp"), P("sp", "tp", None)
    return jax.shard_map(
        per_device,
        mesh=mesh,
        in_specs=(
            *(by_position,) * 4,
            *(by_head,) * 3,
            P("sp", "tp"),
            P(None, "tp"),
            columns,
            columns,
            rows,
        ),
        out_specs=(columns, columns, rows, P("sp", "tp"), *(by_head,) * 3),
        check_vma=False,
    )
```

time: 404 us -> 107 us (0.26)
  waiting for transfers between devices: 177 us -> 0 us
  Pallas kernels: 0 us -> 106 us
  blocking collectives: 67.4 us -> 0 us
  local copies, waits for them, and re-layouts: 39.3 us -> 0 us
  other arithmetic: 35.3 us -> 0 us
  matrix products: 34.4 us -> 0 us
  starting transfers between devices: 32.4 us -> 0 us
  between operations: 15.3 us -> 0.81 us
    pallas_call x0 -> x2, Pallas kernels: none -> 106 us  [the longest x1 104 us: per_device(): pl.pallas_call(kernel, out_shape=tuple((pltpu.VMEM(*o) for o in OUTPUTS.v...]
    all_to_all x4 -> x0, waiting for transfers between devices: 105 us -> none  [the longest x1 73.2 us: in_one_piece(): lax.all_to_all(both, axis, split_axis=split_dim, concat_axis=concat_dim,...]
    all_gather x7 -> x0, blocking collectives: 64.9 us -> none  [the longest x4 37.9 us: prefix_by_axis(): lax.all_gather(part.astype(kind), axis)]
    reduce_scatter x3 -> x0, waiting for transfers between devices: 39.3 us -> none  [summed_rows(): total = lax.psum_scatter(total, axis, scatter_dimension=0, tiled=True)]
    dot_general x22 -> x0, matrix products: 34.4 us -> none  [the longest x1 3.48 us: expert_local(): lax.dot_general(activated, routed_grads, (((0,), (0,)), ((), ())), prefer...]
    all_gather x2 -> x0, waiting for transfers between devices: 33.1 us -> none  [the longest x1 33.1 us: prefix_by_axis_2(): lax.all_gather(part.astype(kind), axis)]
    all_to_all x4 -> x0, starting transfers between devices: 31.7 us -> none  [the longest x1 12.4 us: in_one_piece(): lax.all_to_all(both, axis, split_axis=split_dim, concat_axis=concat_dim,...]
    gather x4 -> x0, local copies, waits for them, and re-layouts: 12.4 us -> none  [the longest x2 5.86 us: per_device(): jnp.take(returned, destination, axis=0).reshape(tokens_here, 2, model_width)]
  transfers between devices with their start and end apart: 9 -> 0, of which waited for: 7 -> 0; matrix products, arithmetic and copies ran while one was open for 14% -> 0% of each run, Pallas kernels for 0% -> 0%
where the time goes in v2:
time: 107 us
  Pallas kernels  106 us (99%)
    pallas_call x1, Pallas kernels, per_device(): pl.pallas_call(kernel, out_shape=tuple((pltpu.VMEM(*o) for o in OUTPUTS.v...  104 us

profile of v2, /device:TPU:33, one launch (start us, length us, event | category | flops | bytes accessed | tf_op | source)
XLA Modules:
  0.0 106.6 jit_solution(7990184894627172407)
XLA Ops:
  0.6 104.0 %shard_map.189 = (bf16[1,2048,256]{2,1,0:T(8,128)(2,1)S(1)}, bf16[1,2048,256]{2,1,0:T(8,128)(2,1)S(1)}, bf16[1,256,2048]{2,1,0:T(8,128)(2,1)S(1)}, f32[32,512]{1...) custom-call(bf16[128,2048]{1,0:T(8,128)(2,1)} %refs_0_.1, ...), custom_call_target="tpu_custom_call" | custom-call | tf_op jit(solution)/shard_map/pallas_call | solution.py:784
  104.6 1.8 %shard_map.190 = (bf16[1,2048,256]{2,1,0:T(8,128)(2,1)}, bf16[1,2048,256]{2,1,0:T(8,128)(2,1)}, bf16[1,256,2048]{2,1,0:T(8,128)(2,1)}, f32[32,512]{1,0:T(8,128)}...) custom-call(bf16[1,2048,256]{2,1,0:T(8,128)(2,1)S(1)} %get-tuple-element.14.refs_0_, ...), custom_call_target="tpu_custom_call" | custom-call | tf_op jit(solution)/shard_map/pallas_call | solution.py:812

commit v3 on v2

--- a/solution.py
+++ b/solution.py
@@ -109,6 +109,16 @@
     "o_key": ((TOK, 2, KD), BF),
     "o_value": ((TOK, 2, VD), BF),
 }
+LEFT = {
+    **dict(list(OUTPUTS.items())[:5]),
+    "kr": ((2, TOK, KD), F32),
+    "vh": ((2, TOK, VD), BF),
+    "rem": ((2, TOK, 1), F32),
+    "kpart": ((2, TOK, KD), F32),
+    "vpart": ((2, TOK, VD), F32),
+    "future": ((2, KD, VD), BF),
+    "turns": ((2, TOK, KD), F32),
+}
 BUFFERS = {
     **SMALL,
     "sf": ((TOK, D), BF),
@@ -130,14 +140,11 @@
     "ret": ((N_SP, 8, QUART), BF),
     "rt": ((N_SP, 32, TOK), BF),
     "qr": ((2, TOK, KD), F32),
-    "kr": ((2, TOK, KD), F32),
-    "vh": ((2, TOK, VD), BF),
     "mask": ((2, TOK, TOK), F32),
     "wt": ((2, TOK, TOK), BF),
     "nrm": ((2, TOK, VD), F32),
     "inv": ((2, TOK, 1), F32),
     "phd": ((2, TOK, 1), F32),
-    "rem": ((2, TOK, 1), F32),
     "sa": ((2, 8, 32, VD), BF),
     "ra": ((2, 8, 32, VD), BF),
     "pp": ((2, 8, 32, VD), F32),
@@ -145,6 +152,7 @@
     "rb": ((2, 8, 32, VD), BF),
     "sc": ((2, 8, 32, VD), BF),
     "rc": ((2, 8, 32, VD), BF),
+    "run": ((32, VD), F32),
     "tmine": ((2, VD), F32),
     "tplane": ((2, VD), F32),
     "ta": ((8, 2, VD), F32),
@@ -169,6 +177,8 @@
     "g_recv": (6,),
     "s_send": (2, 3),
     "s_recv": (2, 3),
+    "b_send": (2, 8),
+    "b_recv": (2, 8),
     "u_send": (2,),
     "u_recv": (2,),
     "n_send": (),
@@ -177,7 +187,22 @@
     "p_recv": (),
     "q_recv": (4,),
 }
-NAMES = (*INPUTS, *OUTPUTS, *BUFFERS, *SEMAPHORES)
+NAMES = (*INPUTS, *LEFT, *BUFFERS, *SEMAPHORES)
+
+
+def turn(field, cosines, sines):
+    odd = iota((TOK, KD), 1) % 2 == 1
+    partner = jnp.where(odd, pltpu.roll(field, 1, 1), pltpu.roll(field, KD - 1, 1))
+    return field * cosines + partner * sines
+
+
+def apart():
+    a, b = iota((256, 256), 0), iota((256, 256), 1)
+    return (b == 2 * (a % 128) + a // 128).astype(BF)
+
+
+def together(parts):
+    return dot(apart(), jnp.concatenate(parts, axis=0).astype(BF), 0, 0).astype(BF)
 
 
 def kernel(*refs):
@@ -292,17 +317,10 @@
         cb, sb = r.places[0:128, :], r.places[128:256, :]
         return ca * cb - sa * sb, jnp.where(odd, 1.0, -1.0) * (sa * cb + ca * sb)
 
-    def turn(field, cosines, sines):
-        partner = jnp.where(odd, pltpu.roll(field, 1, 1), pltpu.roll(field, TOK - 1, 1))
-        return field * cosines + partner * sines
-
-    def apart():
-        a, b = iota((256, 256), 0), iota((256, 256), 1)
-        return (b == 2 * (a % 128) + a // 128).astype(BF)
-
     for c in loads[4:10]:
         c.wait()
     cosines, sines = angles()
+    r.turns[0], r.turns[1] = cosines, sines
     split = apart()
     q2 = dot(split, r.queries[...].reshape(256, KD), 1, 0)
     k2 = dot(split, r.keys[...].reshape(256, KD), 1, 0)
@@ -370,26 +388,35 @@
             r.pp[way, m] = run
             run = jnp.exp(r.ta[m, head, :]) * run + r.ra[way, m].astype(F32)
         r.sb[way] = run.astype(BF)
-        over_z(
-            lambda p: r.sb.at[way],
-            lambda p: r.rb.at[way, p],
-            r.s_send.at[way, 1],
-            r.s_recv.at[way, 1],
-        )
-        r.rb[way, z] = r.sb[way]
+        for dz in PARTS:
+            p = plane(dz)
+
+            @pl.when((p > z) if way == 0 else (p < z))
+            def _(p=p):
+                remote(
+                    r.sb.at[way],
+                    r.rb.at[way, z],
+                    r.b_send.at[way, p],
+                    r.b_recv.at[way, z],
+                    (p * 8 + j, x),
+                )
+
         if way == 0:
             over_z(lambda p: r.tplane, lambda p: r.tb.at[p], r.u_send.at[1], r.u_recv.at[1])
             r.tb[z] = r.tplane[...]
 
     def stage_c(way):
-        take(r.rb.at[way, pl.ds(0, 7)], r.s_recv.at[way, 1])
         if way == 0:
             take(r.tb.at[pl.ds(0, 7)], r.u_recv.at[1])
-        run = jnp.zeros((32, VD), F32)
+        r.run[...] = jnp.zeros((32, VD), F32)
         for p in range(8) if way == 0 else reversed(range(8)):
-            passed = (p < z) if way == 0 else (p > z)
-            new = jnp.exp(r.tb[p, head, :]) * run + r.rb[way, p].astype(F32)
-            run = jnp.where(passed, new, run)
+
+            @pl.when((p < z) if way == 0 else (p > z))
+            def _(p=p):
+                take(r.rb.at[way, p], r.b_recv.at[way, p])
+                r.run[...] = jnp.exp(r.tb[p, head, :]) * r.run[...] + r.rb[way, p].astype(F32)
+
+        run = r.run[...]
         logs = jnp.zeros((1, VD), F32)
         for m in range(8) if way == 0 else reversed(range(8)):
             r.sc[way, m] = (jnp.exp(logs) * run + r.pp[way, m]).astype(BF)
@@ -417,6 +444,8 @@
             r.nrm[h] = kept * inv
             r.nb[:, 256 * h : 256 * h + 256] = (kept * inv).astype(BF)
         r.na[j] = r.nb[...]
+
+    def share_normed():
         remote(r.nb, r.na.at[j], r.n_send, r.n_recv.at[0], (z * 8 + other, x))
         for k in range(1, 4):
             m = (j + 2 * k) % 8
@@ -605,7 +634,7 @@
     forward(4)
     weight_grads(1)
     finish(4)
-    relay()
+    share_normed()
     weight_grads(2)
     weight_grads(3)
 
@@ -651,12 +680,37 @@
     remote(part_of(right, 1), part_of(right, 1), r.g_send, r.g_recv.at[5], (me, left))
     take(part_of(left, 1), r.g_recv.at[2])
     take(part_of(right, 0), r.g_recv.at[3])
+    relay()
     give(1, left)
     give(2, right)
     normed_grad = share(x) + share(left) + share(right)
     take(part_of(far, 0), r.g_recv.at[4])
     take(part_of(far, 1), r.g_recv.at[5])
     normed_grad = normed_grad + share(far)
+
+    def project(*pieces):
+        for i, _ in pieces:
+            take(r.rt.at[pl.ds(0, 14)], r.q_recv.at[i])
+
+        def rows_of(m):
+            return jnp.concatenate(
+                [r.rr[m, pl.ds(2 * q, 2)].reshape(64, TOK) for _, q in pieces], axis=0
+            )
+
+        part = dot(rows_of(0), r.na[0], 1, 0)
+        for m in range(1, 8):
+            part = part + dot(rows_of(m), r.na[m], 1, 0)
+        for k, (_, q) in enumerate(pieces):
+            r.zp[pl.ds(2 * q, 2)] = part[64 * k : 64 * k + 64].astype(BF).reshape(2, 32, 512)
+            for to in (2 * q, 2 * q + 1):
+
+                @pl.when(to != z)
+                def _(to=to):
+                    remote(r.zp.at[to], r.rz.at[z], r.p_send.at[1], r.p_recv, (to * 8 + j, x))
+
+                @pl.when(to == z)
+                def _():
+                    r.rz[z] = r.zp[z]
 
     grads = []
     for h in range(2):
@@ -668,48 +722,22 @@
         r.sa[1, pl.ds(4 * h, 4)] = inner.astype(BF).reshape(4, 32, VD)
     stage_a(1)
     give(3, far)
-
-    query_parts, key_parts, value_parts = [], [], []
+    take(r.nb, r.n_recv.at[0])
+    take(r.na.at[pl.ds(0, 3)], r.n_recv.at[2])
+    project((0, x))
+
+    query_parts = []
     for h in range(2):
         q, k, v, g = r.qr[h], r.kr[h], r.vh[h], grads[h]
         score = (dot(g, v, 1, 1) * r.mask[h]).astype(BF)
         query_parts.append(dotb(score, k, 1, 0) + r.phd[h] * dot(g, state_of(0, h), 1, 1))
-        key_parts.append(dotb(score, q, 0, 0))
-        value_parts.append(dot(r.wt[h], g, 0, 0))
-
-    def together(parts):
-        return dot(split, jnp.concatenate(parts, axis=0).astype(BF), 0, 0).astype(BF)
+        r.kpart[h] = dotb(score, q, 0, 0)
+        r.vpart[h] = dot(r.wt[h], g, 0, 0)
 
     r.o_query[...] = together([turn(p, cosines, -sines) for p in query_parts]).reshape(TOK, 2, KD)
 
-    def project(*pieces):
-        for i, _ in pieces:
-            take(r.rt.at[pl.ds(0, 14)], r.q_recv.at[i])
-
-        def rows_of(m):
-            return jnp.concatenate(
-                [r.rr[m, pl.ds(2 * q, 2)].reshape(64, TOK) for _, q in pieces], axis=0
-            )
-
-        part = dot(rows_of(0), r.na[0], 1, 0)
-        for m in range(1, 8):
-            part = part + dot(rows_of(m), r.na[m], 1, 0)
-        for k, (_, q) in enumerate(pieces):
-            r.zp[pl.ds(2 * q, 2)] = part[64 * k : 64 * k + 64].astype(BF).reshape(2, 32, 512)
-            for to in (2 * q, 2 * q + 1):
-
-                @pl.when(to != z)
-                def _(to=to):
-                    remote(r.zp.at[to], r.rz.at[z], r.p_send.at[1], r.p_recv, (to * 8 + j, x))
-
-                @pl.when(to == z)
-                def _():
-                    r.rz[z] = r.zp[z]
-
     stage_b(1)
-    take(r.nb, r.n_recv.at[0])
-    take(r.na.at[pl.ds(0, 3)], r.n_recv.at[2])
-    project((0, x), (1, left), (2, right), (3, far))
+    project((1, left), (2, right), (3, far))
     stage_c(1)
 
     take(r.rz.at[pl.ds(0, 7)], r.p_recv)
@@ -720,15 +748,7 @@
 
     take(r.rc.at[1, pl.ds(0, 7)], r.s_recv.at[1, 2])
     for h in range(2):
-        future = state_of(1, h)
-        key_parts[h] = key_parts[h] + r.rem[h] * dot(r.vh[h], future, 1, 1)
-        value_parts[h] = value_parts[h] + r.rem[h] * dotb(r.kr[h], future, 1, 0)
-    r.o_key[...] = together(
-        [turn(p, cosines, -sines) * KD ** (-0.5) for p in key_parts]
-    ).reshape(TOK, 2, KD)
-    for i in range(2):
-        at = slice(128 * i, 128 * i + 128)
-        r.o_value[:, :, at] = together([p[:, at] for p in value_parts]).reshape(TOK, 2, 128)
+        r.future[h] = state_of(1, h)
 
     take(r.rg.at[pl.ds(0, 27)], r.d_send)
     take(r.rg.at[pl.ds(0, 36)], r.x_send)
@@ -737,7 +757,12 @@
     take(r.rt.at[pl.ds(0, 48)], r.g_send)
     for way in range(2):
         take(r.sa.at[way, pl.ds(0, 7)], r.s_send.at[way, 0])
-        take(r.rb.at[way, pl.ds(0, 7)], r.s_send.at[way, 1])
+        for p in range(8):
+
+            @pl.when((p > z) if way == 0 else (p < z))
+            def _(p=p):
+                take(r.sb.at[way], r.b_send.at[way, p])
+
         take(r.sc.at[way, pl.ds(0, 7)], r.s_send.at[way, 2])
     take(r.ta.at[pl.ds(0, 7)], r.u_send.at[0])
     take(r.tb.at[pl.ds(0, 7)], r.u_send.at[1])
@@ -746,11 +771,26 @@
     take(r.zp.at[pl.ds(0, 7)], r.p_send.at[1])
 
 
-def write_out(*refs):
-    n = len(OUTPUTS)
-    copies = [pltpu.make_async_copy(refs[i], refs[n + i], refs[2 * n].at[i]) for i in range(n)]
-    for c in copies:
+def last_step(*refs):
+    n, m = len(LEFT), len(OUTPUTS)
+    r = types.SimpleNamespace(**dict(zip(LEFT, refs[:n], strict=True)))
+    outs, (key, value, sems) = refs[n : n + m], refs[n + m :]
+    ready = [*refs[:5], key, value]
+    copies = [pltpu.make_async_copy(ready[i], outs[i], sems.at[i]) for i in range(m)]
+    for c in copies[:5]:
         c.start()
+    cosines, sines = r.turns[0], r.turns[1]
+    keys, values = [], []
+    for h in range(2):
+        k = r.kpart[h] + r.rem[h] * dot(r.vh[h], r.future[h], 1, 1)
+        keys.append(turn(k, cosines, -sines) * KD ** (-0.5))
+        values.append(r.vpart[h] + r.rem[h] * dotb(r.kr[h], r.future[h], 1, 0))
+    key[...] = together(keys).reshape(TOK, 2, KD)
+    copies[5].start()
+    for i in range(2):
+        at = slice(128 * i, 128 * i + 128)
+        value[:, :, at] = together([v[:, at] for v in values]).reshape(TOK, 2, 128)
+    copies[6].start()
     for c in copies:
         c.wait()
 
@@ -783,15 +823,15 @@
     local = pl.BlockSpec(memory_space=pltpu.VMEM)
     results = pl.pallas_call(
         kernel,
-        out_shape=tuple(pltpu.VMEM(*o) for o in OUTPUTS.values()),
+        out_shape=tuple(pltpu.VMEM(*o) for o in LEFT.values()),
         in_specs=(anywhere,) * len(INPUTS),
-        out_specs=(local,) * len(OUTPUTS),
+        out_specs=(local,) * len(LEFT),
         scratch_shapes=[
             *(pltpu.VMEM(*b) for b in BUFFERS.values()),
             *(pltpu.SemaphoreType.DMA(s) if s else pltpu.SemaphoreType.DMA for s in SEMAPHORES.values()),
         ],
         compiler_params=pltpu.CompilerParams(
-            collective_id=0, has_side_effects=True, vmem_limit_bytes=60 * 1024 * 1024
+            collective_id=0, has_side_effects=True, vmem_limit_bytes=62_600_000
         ),
     )(
         stream,
@@ -810,12 +850,16 @@
         jnp.asarray(places),
     )
     return pl.pallas_call(
-        write_out,
+        last_step,
         out_shape=tuple(jax.ShapeDtypeStruct(*o) for o in OUTPUTS.values()),
-        in_specs=(local,) * len(OUTPUTS),
+        in_specs=(local,) * len(LEFT),
         out_specs=(anywhere,) * len(OUTPUTS),
-        scratch_shapes=[pltpu.SemaphoreType.DMA((len(OUTPUTS),))],
-        compiler_params=pltpu.CompilerParams(vmem_limit_bytes=1024 * 1024),
+        scratch_shapes=[
+            pltpu.VMEM((TOK, 2, KD), BF),
+            pltpu.VMEM((TOK, 2, VD), BF),
+            pltpu.SemaphoreType.DMA((len(OUTPUTS),)),
+        ],
+        compiler_params=pltpu.CompilerParams(vmem_limit_bytes=8 * 1024 * 1024),
     )(*(pltpu.with_memory_space_constraint(a, pltpu.VMEM) for a in results))
 
 

time: 107 us -> 107 us (level)
  no operation moved by 1% of the time
where the time goes in v3:
time: 107 us
  Pallas kernels  106 us (99%)
    pallas_call x1, Pallas kernels, per_device(): pl.pallas_call(kernel, out_shape=tuple((pltpu.VMEM(*o) for o in LEFT.valu...  104 us

profile of v3, /device:TPU:33, one launch (start us, length us, event | category | flops | bytes accessed | tf_op | source)
XLA Modules:
  0.0 106.7 jit_solution(9655375917861971857)
XLA Ops:
  0.6 104.0 %shard_map.189 = (bf16[1,2048,256]{2,1,0:T(8,128)(2,1)S(1)}, bf16[1,2048,256]{2,1,0:T(8,128)(2,1)S(1)}, bf16[1,256,2048]{2,1,0:T(8,128)(2,1)S(1)}, f32[32,512]{1...) custom-call(bf16[128,2048]{1,0:T(8,128)(2,1)} %refs_0_.1, ...), custom_call_target="tpu_custom_call" | custom-call | tf_op jit(solution)/shard_map/pallas_call | solution.py:824
  104.7 1.9 %shard_map.190 = (bf16[1,2048,256]{2,1,0:T(8,128)(2,1)}, bf16[1,2048,256]{2,1,0:T(8,128)(2,1)}, bf16[1,256,2048]{2,1,0:T(8,128)(2,1)}, f32[32,512]{1,0:T(8,128)}...) custom-call(bf16[1,2048,256]{2,1,0:T(8,128)(2,1)S(1)} %get-tuple-element.19.refs_0_, ...), custom_call_target="tpu_custom_call" | custom-call | tf_op jit(solution)/shard_map/pallas_call | solution.py:852
